TPU v7x, 32 devices: a whole 2x2x4 slice. The times are simulated.
32 devices in a mesh: sp: 8 (over z, x), tp: 4 (over y, core).
Axes of the slice: x: 2, y: 2, z: 4, core: 2. Of those that a mesh axis runs over, the one named last changes fastest.
Arguments:
- outer_gate: bfloat16 [2048, 2048], P('sp', 'tp'), may hold values from -6 to 6
- inner_gate: bfloat16 [2048, 2048], P('sp', 'tp'), may hold values from -6 to 6
- conv_input: bfloat16 [2048, 2048], P('sp', 'tp'), may hold values from -6 to 6
- conv_weight: bfloat16 [3, 2048], P(None, 'tp'), may hold values from -3.5 to 3.5
- doc_ids: int32 [2048], P('sp'), may hold values from 0 to 3, as said below
- output_weight: bfloat16 [2048, 4096], P(None, 'tp'), may hold values from -0.125 to 0.125
- residual: bfloat16 [2048, 4096], P('sp', 'tp'), as said below
- norm_gain: bfloat16 [4096], P('tp'), may hold values from 0.099609375 to 1.8984375
- expert_ids: int32 [2048, 2], P('sp'), may hold values from 0 to 7, all different within a row; in each aligned block of 256 rows (0 to 255, 256 to 511, ...) at most 128 rows name the same one
- group_weight: float32 [2048], P('sp'), may hold values from 0.25 to 1
- expert_weight: float32 [2048, 2], P('sp'), may hold values from 0.05 to 1
- gate_weight: bfloat16 [8, 4096, 2048], P('sp', None, 'tp'), may hold values from -0.09375 to 0.09375
- up_weight: bfloat16 [8, 4096, 2048], P('sp', None, 'tp'), may hold values from -0.09375 to 0.09375
- down_weight: bfloat16 [8, 2048, 4096], P('sp', None, 'tp'), may hold values from -0.125 to 0.125
Outputs:
- layer_out: bfloat16 [2048, 4096], P('sp', 'tp')
Inputs may be any that keep to these rules, and one draw needn't show every extreme that they name: `expert_ids`: within the 256 rows of one index of sp no expert is named more than 128 times, a bound that some block reaches; the two experts of a row differ. `doc_ids`: never falling along positions, rising by one at each document's start; every document has 256 to 768 positions, and one exactly 768. `residual`: Columns' scales are of order one to ten.
All inputs are finite; a program needn't handle non-finite values.
Results may differ from a plain program's by a relative error of at most 0.009.
Values may be sent and summed in bfloat16 or wider, within the bound.
A program may use at most 64 MiB of HBM per device.

v0:
```python
import functools

import jax
import jax.numpy as jnp
from jax import lax
from jax.experimental import pallas as pl
from jax.experimental.pallas import tpu as pltpu
from jax.sharding import PartitionSpec as P

EPS = 1e-06
MESH = pl.DeviceIdType.MESH


def remote(src, dst, send_sem, recv_sem, device):
    return pltpu.make_async_remote_copy(
        src_ref=src,
        dst_ref=dst,
        send_sem=send_sem,
        recv_sem=recv_sem,
        device_id=device,
        device_id_type=MESH,
    )


def expert_kernel(
    n,
    tp,
    outer_ref,
    inner_ref,
    conv_ref,
    taps_ref,
    docs_ref,
    residual_ref,
    gain_ref,
    ids_ref,
    mix_ref,
    proj_hbm,
    gate_hbm,
    up_hbm,
    down_hbm,
    result_ref,
    out_ref,
    ret_ref,
    branch,
    proj_w,
    acc,
    resid,
    normed,
    squares,
    key_col,
    key_row,
    mix_col,
    halo_inner,
    halo_conv,
    halo_docs,
    piece,
    hid,
    eo,
    gate_w,
    up_w,
    down_w,
    w_sem,
    own_sem,
    a_send,
    a_recv,
    y_send,
    y_recv,
    p_send,
    p_recv,
    hy_send,
    hy_recv,
    hp_send,
    hp_recv,
    r_send,
    r_recv,
    h_send,
    h_recv,
    by_send,
    by_recv,
    bp_send,
    bp_recv,
    s_send,
    s_recv,
):
    me = lax.axis_index("sp")
    t = lax.axis_index("tp")
    chips = tp // 2
    y, core = lax.div(t, 2), lax.rem(t, 2)
    partner = t + 1 - 2 * core
    cap, cols = out_ref.shape[1], out_ref.shape[2]
    ffn_local = gate_w.shape[1]
    groups, group_rows = hid.shape[0], hid.shape[1]
    fans = p_send.shape[1]
    fan_blocks = n // fans
    group_fans = fans // groups
    group_blocks = n // groups

    def column(index, width):
        return pl.ds(pl.multiple_of(index * width, 128), width)

    def chip_at(delta):
        return lax.rem(y + delta + chips, chips) * 2 + core

    weight_copies = [
        pltpu.make_async_copy(source, target, w_sem.at[i])
        for i, (source, target) in enumerate(
            (
                (gate_hbm.at[0], gate_w),
                (up_hbm.at[0], up_w),
                (down_hbm.at[0], down_w),
                (proj_hbm, proj_w),
            )
        )
    ]
    for i in (3, 0, 1, 2):
        weight_copies[i].start()

    barrier = pltpu.get_barrier_semaphore()
    for k in range(1, n):
        pl.semaphore_signal(
            barrier, inc=1, device_id=(lax.rem(me + k, n), t), device_id_type=MESH
        )
    for d in range(1, tp):
        pl.semaphore_signal(
            barrier, inc=1, device_id=(me, lax.rem(t + d, tp)), device_id_type=MESH
        )
    pl.semaphore_wait(barrier, n - 1 + tp - 1)

    sends = []
    arrivals = []
    row_count = residual_ref.shape[0]
    wide = branch.shape[1] // tp

    halos = []
    following = (lax.rem(me + 1, n), t)
    for i, (source, target) in enumerate(
        (
            (inner_ref.at[pl.ds(row_count - 16, 16)], halo_inner),
            (conv_ref.at[pl.ds(row_count - 16, 16)], halo_conv),
            (docs_ref.at[pl.ds(row_count - 8, 8)], halo_docs),
        )
    ):
        copy = remote(source, target, h_send.at[i], h_recv.at[i], following)
        copy.start()
        halos.append(copy)
        sends.append(copy)

    lanes = lax.broadcasted_iota(jnp.int32, (row_count, 128), 1)
    first_id, second_id = ids_ref[:, 0:1], ids_ref[:, 1:2]
    is_first, is_second = lanes == first_id, lanes == second_id
    mix_col[...] = jnp.where(is_first, mix_ref[:, 0:1], 0.0) + jnp.where(
        is_second, mix_ref[:, 1:2], 0.0
    )
    member = jnp.where(is_first, 1.0, 0.0) + jnp.where(is_second, 1.0, 0.0)
    earlier = jnp.where(
        lax.broadcasted_iota(jnp.int32, (row_count, row_count), 1)
        < lax.broadcasted_iota(jnp.int32, (row_count, row_count), 0),
        1.0,
        0.0,
    ).astype(jnp.bfloat16)
    ranks = jnp.dot(earlier, member.astype(jnp.bfloat16), preferred_element_type=jnp.float32)
    keys = jnp.where(member > 0.5, ranks, -1.0)
    key_col[...] = keys
    key_row[...] = keys.T

    for copy in halos:
        copy.wait_recv()
    row_at = lax.broadcasted_iota(jnp.int32, (row_count, 1), 0)
    own_docs = docs_ref[:, 0:1]
    halo_ids = jnp.where(me > 0, halo_docs[...], -1.0)[:, 0:1]
    docs_one = jnp.where(row_at == 0, halo_ids[7:8], pltpu.roll(docs_ref[...], 1, 0)[:, 0:1])
    docs_two = jnp.where(
        row_at == 0,
        halo_ids[6:7],
        jnp.where(row_at == 1, halo_ids[7:8], pltpu.roll(docs_ref[...], 2, 0)[:, 0:1]),
    )
    same_one, same_two = docs_one == own_docs, docs_two == own_docs

    def conv_tile(j, carry):
        at = pl.ds(pl.multiple_of(j * 128, 128), 128)
        products = inner_ref[:, at].astype(jnp.float32) * conv_ref[:, at].astype(jnp.float32)
        before = halo_inner[:, at].astype(jnp.float32) * halo_conv[:, at].astype(jnp.float32)
        one = jnp.where(row_at == 0, before[15:16], pltpu.roll(products, 1, 0))
        two = jnp.where(
            row_at == 0,
            before[14:15],
            jnp.where(row_at == 1, before[15:16], pltpu.roll(products, 2, 0)),
        )
        taps = taps_ref[:, at].astype(jnp.float32)
        conv = taps[2:3] * products
        conv = conv + jnp.where(same_one, taps[1:2] * one, 0.0)
        conv = conv + jnp.where(same_two, taps[0:1] * two, 0.0)
        value = (outer_ref[:, at].astype(jnp.float32) * conv).astype(jnp.bfloat16)
        branch[:, pl.ds(pl.multiple_of(t * wide + j * 128, 128), 128)] = value
        return carry

    lax.fori_loop(0, wide // 128, conv_tile, 0)

    def branch_region(index):
        return branch.at[:, column(index, wide)]

    region = branch_region(t)
    for d in range(1, chips):
        copy = remote(region, region, by_send.at[d], by_recv.at[d], (me, chip_at(d)))
        copy.start()
        sends.append(copy)
    copy = remote(region, region, bp_send.at[0], bp_recv.at[0], (me, partner))
    copy.start()
    sends.append(copy)
    weight_copies[3].wait()

    def project(index, first=False):
        step = min(256, cols)

        def tile(j, carry):
            at = pl.ds(pl.multiple_of(j * step, 128), step)
            rows = pl.ds(pl.multiple_of(index * wide, 128), wide)
            value = jnp.dot(
                branch[:, column(index, wide)], proj_w[rows, at], preferred_element_type=jnp.float32
            )
            acc[:, at] = value if first else acc[:, at] + value
            return carry

        lax.fori_loop(0, cols // step, tile, 0)

    project(t, True)
    other = branch_region(partner)
    remote(other, other, bp_send.at[0], bp_recv.at[0], (me, partner)).wait_recv()
    project(partner)
    for d in range(1, chips):
        source = chip_at(-d)
        region = branch_region(source)
        remote(region, region, by_send.at[d], by_recv.at[d], (me, partner)).wait_recv()
        copy = remote(region, region, bp_send.at[d], bp_recv.at[d], (me, partner))
        copy.start()
        sends.append(copy)
        project(source)
    for d in range(1, chips):
        source = chip_at(-d) + partner - t
        region = branch_region(source)
        remote(region, region, bp_send.at[d], bp_recv.at[d], (me, partner)).wait_recv()
        project(source)

    def resid_tile(j, total):
        at = pl.ds(pl.multiple_of(j * 128, 128), 128)
        value = (residual_ref[:, at].astype(jnp.float32) + acc[:, at]).astype(jnp.bfloat16)
        resid[:, at] = value
        value = value.astype(jnp.float32)
        return total + value * value

    total = lax.fori_loop(
        0, cols // 128, resid_tile, jnp.zeros((row_count, 128), jnp.float32)
    )
    squares[t] = jnp.broadcast_to(
        jnp.sum(total.T, axis=0, keepdims=True), (8, row_count)
    )
    for d in range(1, tp):
        copy = remote(
            squares.at[t], squares.at[t], s_send.at[d], s_recv.at[d], (me, lax.rem(t + d, tp))
        )
        copy.start()
        sends.append(copy)
    for d in range(1, tp):
        source = lax.rem(t + tp - d, tp)
        remote(
            squares.at[source], squares.at[source], s_send.at[d], s_recv.at[d], (me, source)
        ).wait_recv()
    total_sq = jnp.sum(squares[...], axis=0)[0:1]
    scale_row = lax.rsqrt(total_sq / (tp * cols) + EPS)
    scale = jnp.broadcast_to(scale_row, (128, row_count)).T

    def norm_tile(j, carry):
        at = pl.ds(pl.multiple_of(j * 128, 128), 128)
        value = resid[:, at].astype(jnp.float32) * scale * gain_ref[:, at].astype(jnp.float32)
        normed[:, at] = value.astype(jnp.bfloat16)
        return carry

    lax.fori_loop(0, cols // 128, norm_tile, 0)

    slot_rows = lax.broadcasted_iota(jnp.int32, (cap, row_count), 0).astype(jnp.float32)

    def choose(expert):
        select = jnp.where(slot_rows == key_row[pl.ds(expert, 1), :], 1.0, 0.0)
        out_ref[expert] = jnp.dot(
            select.astype(jnp.bfloat16), normed[...], preferred_element_type=jnp.float32
        ).astype(jnp.bfloat16)

    for k in range(1, n):
        there = lax.rem(me + k, n)
        choose(there)
        copy = remote(
            out_ref.at[there],
            piece.at[k, :, column(t, cols)],
            a_send.at[k],
            a_recv.at[k],
            (there, t),
        )
        copy.start()
        sends.append(copy)
        arrivals.append(copy)
    choose(me)
    own_in = pltpu.make_async_copy(out_ref.at[me], piece.at[0, :, column(t, cols)], own_sem.at[0])
    own_in.start()

    def fan_region(f, index):
        return piece.at[pl.ds(f * fan_blocks, fan_blocks), :, column(index, cols)]

    def fan_out(f):
        for k in range(f * fan_blocks, (f + 1) * fan_blocks):
            if k == 0:
                own_in.wait()
            else:
                arrivals[k - 1].wait_recv()
        region = fan_region(f, t)
        for d in range(1, chips):
            copy = remote(
                region, region, y_send.at[d, f], y_recv.at[d, f], (me, chip_at(d))
            )
            copy.start()
            sends.append(copy)
        copy = remote(region, region, p_send.at[0, f], p_recv.at[0, f], (me, partner))
        copy.start()
        sends.append(copy)

    def relay(f):
        for d in range(1, chips):
            source = chip_at(-d)
            region = fan_region(f, source)
            remote(
                region, region, y_send.at[d, f], y_recv.at[d, f], (me, partner)
            ).wait_recv()
            copy = remote(region, region, p_send.at[d, f], p_recv.at[d, f], (me, partner))
            copy.start()
            sends.append(copy)

    def hid_region(g, index):
        return hid.at[g, :, column(index, ffn_local)]

    def up_stage(g):
        for f in range(g * group_fans, (g + 1) * group_fans):
            for d in range(chips):
                region = fan_region(f, chip_at(-d) + partner - t)
                remote(
                    region, region, p_send.at[d, f], p_recv.at[d, f], (me, partner)
                ).wait_recv()
        if g == 0:
            weight_copies[0].wait()
            weight_copies[1].wait()
        step = min(256, ffn_local)

        def tile(j, carry):
            rows = piece[pl.ds(g * group_blocks, group_blocks)].reshape(group_rows, tp * cols)
            at = pl.ds(pl.multiple_of(j * step, 128), step)
            gate_val = jnp.dot(rows, gate_w[:, at], preferred_element_type=jnp.float32)
            up_val = jnp.dot(rows, up_w[:, at], preferred_element_type=jnp.float32)
            hidden = (jax.nn.silu(gate_val) * up_val).astype(jnp.bfloat16)
            hid[g, :, pl.ds(pl.multiple_of(t * ffn_local + j * step, 128), step)] = hidden
            return carry

        lax.fori_loop(0, ffn_local // step, tile, 0)
        region = hid_region(g, t)
        for d in range(1, chips):
            copy = remote(
                region, region, hy_send.at[d, g], hy_recv.at[d, g], (me, chip_at(d))
            )
            copy.start()
            sends.append(copy)
        copy = remote(region, region, hp_send.at[0, g], hp_recv.at[0, g], (me, partner))
        copy.start()
        sends.append(copy)

    def relay_hidden(g):
        for d in range(1, chips):
            region = hid_region(g, chip_at(-d))
            remote(
                region, region, hy_send.at[d, g], hy_recv.at[d, g], (me, partner)
            ).wait_recv()
            copy = remote(region, region, hp_send.at[d, g], hp_recv.at[d, g], (me, partner))
            copy.start()
            sends.append(copy)

    returns = []

    def down_stage(g):
        for d in range(chips):
            region = hid_region(g, chip_at(-d) + partner - t)
            remote(
                region, region, hp_send.at[d, g], hp_recv.at[d, g], (me, partner)
            ).wait_recv()
        if g == 0:
            weight_copies[2].wait()
        step = min(256, cols)

        def tile(j, carry):
            at = pl.ds(pl.multiple_of(j * step, 128), step)
            value = jnp.dot(hid[g], down_w[:, at], preferred_element_type=jnp.float32)
            eo[pl.ds(g * group_blocks, group_blocks), :, at] = value.astype(
                jnp.bfloat16
            ).reshape(group_blocks, cap, step)
            return carry

        lax.fori_loop(0, cols // step, tile, 0)
        for k in range(g * group_blocks, (g + 1) * group_blocks):
            if k == 0:
                copy = pltpu.make_async_copy(eo.at[0], ret_ref.at[me], own_sem.at[1])
            else:
                copy = remote(
                    eo.at[k],
                    ret_ref.at[me],
                    r_send.at[k],
                    r_recv.at[k],
                    (lax.rem(me + n - k, n), t),
                )
            copy.start()
            returns.append(copy)

    def fans_of(g):
        return range(g * group_fans, (g + 1) * group_fans)

    ahead = min(2, groups)
    for g in range(ahead):
        for f in fans_of(g):
            fan_out(f)
    for g in range(groups):
        for f in fans_of(g):
            relay(f)
        up_stage(g)
        if g + ahead < groups:
            for f in fans_of(g + ahead):
                fan_out(f)
        if g >= 1:
            relay_hidden(g - 1)
            down_stage(g - 1)
    relay_hidden(groups - 1)
    down_stage(groups - 1)

    slot_lanes = lax.broadcasted_iota(jnp.int32, (row_count, cap), 1).astype(jnp.float32)
    for g in range(groups):
        members = range(g * group_blocks, (g + 1) * group_blocks)
        for k in members:
            if k == 0:
                returns[0].wait()
            else:
                there = lax.rem(me + k, n)
                returns[k].wait_send()
                remote(
                    eo.at[k], ret_ref.at[there], r_send.at[k], r_recv.at[k], (there, t)
                ).wait_recv()
        chosen = []
        for k in members:
            there = lax.rem(me + k, n)
            here = lanes == there
            key = jnp.sum(jnp.where(here, key_col[...], 0.0), axis=1, keepdims=True)
            weight = jnp.sum(jnp.where(here, mix_col[...], 0.0), axis=1, keepdims=True)
            select = jnp.where(slot_lanes == key, 1.0, 0.0).astype(jnp.bfloat16)
            chosen.append((there, select, weight))
        step = min(256, cols)

        def combine(j, carry):
            at = pl.ds(pl.multiple_of(j * step, 128), step)
            value = jnp.zeros((row_count, step), jnp.float32) if g == 0 else acc[:, at]
            for there, select, weight in chosen:
                value = value + weight * jnp.dot(
                    select, ret_ref[there, :, at], preferred_element_type=jnp.float32
                )
            if g == groups - 1:
                result_ref[:, at] = (resid[:, at].astype(jnp.float32) + value).astype(jnp.bfloat16)
            else:
                acc[:, at] = value
            return carry

        lax.fori_loop(0, cols // step, combine, 0)
    for copy in sends:
        copy.wait_send()


def whole_layer(blocks, weights):
    n, tp = lax.axis_size("sp"), lax.axis_size("tp")
    row_count, wide = blocks[0].shape
    cols = blocks[5].shape[1]
    cap = 4 * row_count // n
    chips = tp // 2
    rows = n * cap
    groups = max(1, min(4, rows // 256))
    fans = min(n, 2 * groups)
    projection, gate_weight, _, down_weight = weights
    width, ffn_local = gate_weight.shape[1], gate_weight.shape[2]
    ffn = down_weight.shape[1]
    dma = pltpu.SemaphoreType.DMA
    bf16, f32 = jnp.bfloat16, jnp.float32
    flops = 2 * rows * width * ffn_local * 2 + 2 * rows * ffn * cols
    return pl.pallas_call(
        functools.partial(expert_kernel, n, tp),
        out_shape=jax.ShapeDtypeStruct((row_count, cols), bf16),
        in_specs=[pl.BlockSpec(memory_space=pltpu.VMEM)] * len(blocks)
        + [pl.BlockSpec(memory_space=pl.ANY)] * len(weights),
        out_specs=pl.BlockSpec(memory_space=pltpu.VMEM),
        scratch_shapes=[
            pltpu.VMEM((n, cap, cols), bf16),
            pltpu.VMEM((n, cap, cols), bf16),
            pltpu.VMEM((row_count, wide * tp), bf16),
            pltpu.VMEM(projection.shape, bf16),
            pltpu.VMEM((row_count, cols), f32),
            pltpu.VMEM((row_count, cols), bf16),
            pltpu.VMEM((row_count, cols), bf16),
            pltpu.VMEM((tp, 8, row_count), f32),
            pltpu.VMEM((row_count, 128), f32),
            pltpu.VMEM((128, row_count), f32),
            pltpu.VMEM((row_count, 128), f32),
            pltpu.VMEM((16, wide), bf16),
            pltpu.VMEM((16, wide), bf16),
            pltpu.VMEM((8, 128), f32),
            pltpu.VMEM((n, cap, width), bf16),
            pltpu.VMEM((groups, rows // groups, ffn), bf16),
            pltpu.VMEM((n, cap, cols), bf16),
            pltpu.VMEM((width, ffn_local), bf16),
            pltpu.VMEM((width, ffn_local), bf16),
            pltpu.VMEM((ffn, cols), bf16),
            dma((4,)),
            dma((2,)),
            dma((n,)),
            dma((n,)),
            dma((chips, fans)),
            dma((chips, fans)),
            dma((chips, fans)),
            dma((chips, fans)),
            dma((chips, groups)),
            dma((chips, groups)),
            dma((chips, groups)),
            dma((chips, groups)),
            dma((n,)),
            dma((n,)),
            dma((3,)),
            dma((3,)),
            dma((chips,)),
            dma((chips,)),
            dma((chips,)),
            dma((chips,)),
            dma((tp,)),
            dma((tp,)),
        ],
        compiler_params=pltpu.CompilerParams(
            collective_id=0, has_side_effects=True, vmem_limit_bytes=56 * 1024 * 1024
        ),
        cost_estimate=pl.CostEstimate(
            flops=flops, bytes_accessed=3 * width * ffn_local * 2, transcendentals=0
        ),
        name="layer",
    )(*blocks, *weights)


def per_device(
    outer_gate,
    inner_gate,
    conv_input,
    conv_weight,
    doc_ids,
    output_weight,
    residual,
    norm_gain,
    expert_ids,
    group_weight,
    expert_weight,
    gate_weight,
    up_weight,
    down_weight,
):
    row_count = conv_input.shape[0]
    docs = jnp.broadcast_to(doc_ids.astype(jnp.float32)[:, None], (row_count, 128))
    mix_weight = (
        group_weight[:, None] * expert_weight / jnp.sum(expert_weight, axis=1, keepdims=True)
    )
    return whole_layer(
        (
            outer_gate,
            inner_gate,
            conv_input,
            conv_weight,
            docs,
            residual,
            norm_gain[None, :],
            expert_ids,
            mix_weight,
        ),
        (output_weight, gate_weight, up_weight, down_weight),
    )


def solution(mesh):
    return jax.shard_map(
        per_device,
        mesh=mesh,
        in_specs=(
            P("sp", "tp"),
            P("sp", "tp"),
            P("sp", "tp"),
            P(None, "tp"),
            P("sp"),
            P(None, "tp"),
            P("sp", "tp"),
            P("tp"),
            P("sp", None),
            P("sp"),
            P("sp", None),
            P("sp", None, "tp"),
            P("sp", None, "tp"),
            P("sp", None, "tp"),
        ),
        out_specs=P("sp", "tp"),
        check_vma=False,
    )
```

profile of v0, /device:TPU:0, one launch (start us, length us, event | category | flops | bytes accessed | tf_op | source)
XLA Modules:
  0.0 149.1 jit_solution(9243183420880017626)
XLA Ops:
  0.0 0.7 convert_element_type.3
  0.7 0.7 fusion
  1.4 1.3 broadcast_in_dim.5.gain_ref
  2.7 0.8 broadcast_in_dim.4.docs_ref
  3.4 0.1 copy.18
  3.6 0.8 broadcast_divide_fusion.mix_ref
  4.3 1.5 copy.20.ids_ref
  5.8 141.4 %layer.1 = bf16[256,1024]{1,0:T(8,128)(2,1)} custom-call(bf16[256,512]{1,0:T(8,128)(2,1)} %outer_ref.1, bf16[256,512]{1,0:T(8,128)(2,1)} %inner_ref.1, bf16[256,512]{1,0:T(8,128)(2,1)} %conv_ref.1, bf16[3,512]{1,0:T(4,128)(2,1)} %taps_ref.1, f32[256,128]{1,0:T(8,128)} %broadcast_in_dim.4.docs_ref, bf16[256,1024]{1,0:T(8,128)(2,1)} %residual_ref.1, ...), custom_call_target="tpu_custom_call" | custom-call | flops 12884901888 | bytes 12582912 | tf_op jit(solution)/shard_map/layer/pallas_call | solution.py:492
  147.2 1.9 %copy.22 = bf16[256,1024]{1,0:T(8,128)(2,1)} copy(bf16[256,1024]{1,0:T(8,128)(2,1)} %layer.1) | data formatting | bytes 1048576
where the time goes:
time: 149 us
  Pallas kernels  141 us (95%)
  local copies, waits for them, and re-layouts  5.5 us (4%)
  other arithmetic  2.14 us (1%)
    pallas_call x1, Pallas kernels, whole_layer(): pl.pallas_call(functools.partial(expert_kernel, n, tp), out_shape=jax.Sha...  141 us
    unnamed x2, local copies, waits for them, and re-layouts  3.34 us

commit v1 on v0

--- a/solution.py
+++ b/solution.py
@@ -25,6 +25,7 @@
 def expert_kernel(
     n,
     tp,
+    across,
     outer_ref,
     inner_ref,
     conv_ref,
@@ -39,16 +40,16 @@
     up_hbm,
     down_hbm,
     result_ref,
-    out_ref,
+    tokens,
+    slots_out,
     ret_ref,
     branch,
     proj_w,
     acc,
     resid,
-    normed,
     squares,
     key_col,
-    key_row,
+    key_rows,
     mix_col,
     halo_inner,
     halo_conv,
@@ -60,9 +61,12 @@
     up_w,
     down_w,
     w_sem,
-    own_sem,
+    k_send,
+    k_recv,
     a_send,
     a_recv,
+    x_send,
+    x_recv,
     y_send,
     y_recv,
     p_send,
@@ -87,13 +91,24 @@
     chips = tp // 2
     y, core = lax.div(t, 2), lax.rem(t, 2)
     partner = t + 1 - 2 * core
-    cap, cols = out_ref.shape[1], out_ref.shape[2]
+    cap, cols = ret_ref.shape[1], ret_ref.shape[2]
     ffn_local = gate_w.shape[1]
-    groups, group_rows = hid.shape[0], hid.shape[1]
-    fans = p_send.shape[1]
-    fan_blocks = n // fans
-    group_fans = fans // groups
-    group_blocks = n // groups
+    depth, group_rows = hid.shape[0], hid.shape[1]
+    z, x = lax.div(me, across), lax.rem(me, across)
+    chunks = a_recv.shape[1]
+    key_count = key_rows.shape[1]
+
+    near = jnp.minimum(z, depth - 1 - z)
+    low = 2 * z < depth
+
+    def group_z(g):
+        if g == 0:
+            return z
+        step = (g + 1) // 2
+        outward = step if g % 2 else -step
+        close = jnp.where(low, z + outward, z - outward)
+        far = jnp.where(low, g, depth - 1 - g)
+        return jnp.where(g <= 2 * near, close, far)
 
     def column(index, width):
         return pl.ds(pl.multiple_of(index * width, 128), width)
@@ -161,7 +176,17 @@
     ranks = jnp.dot(earlier, member.astype(jnp.bfloat16), preferred_element_type=jnp.float32)
     keys = jnp.where(member > 0.5, ranks, -1.0)
     key_col[...] = keys
-    key_row[...] = keys.T
+    key_rows[z] = keys.T[0:key_count]
+    for d in range(1, depth):
+        copy = remote(
+            key_rows.at[z],
+            key_rows.at[z],
+            k_send.at[d],
+            k_recv.at[z],
+            (lax.rem(z + d, depth) * across + x, t),
+        )
+        copy.start()
+        sends.append(copy)
 
     for copy in halos:
         copy.wait_recv()
@@ -272,49 +297,112 @@
     def norm_tile(j, carry):
         at = pl.ds(pl.multiple_of(j * 128, 128), 128)
         value = resid[:, at].astype(jnp.float32) * scale * gain_ref[:, at].astype(jnp.float32)
-        normed[:, at] = value.astype(jnp.bfloat16)
+        tokens[z, :, at] = value.astype(jnp.bfloat16)
         return carry
 
     lax.fori_loop(0, cols // 128, norm_tile, 0)
 
+    chunk = cols // chunks
+    guarded = []
+
+    def token_region(index, c):
+        return tokens.at[index, :, pl.ds(c * chunk, chunk)]
+
+    def pass_on(index, c, sem, target):
+        inside = (target >= 0) & (target < depth)
+        copy = remote(
+            token_region(index, c),
+            token_region(index, c),
+            sem,
+            a_recv.at[index, c],
+            (target * across + x, t),
+        )
+
+        @pl.when(inside)
+        def _():
+            copy.start()
+
+        return inside, copy
+
+    for c in range(chunks):
+        guarded.append(pass_on(z, c, a_send.at[0, c], z + 1))
+        guarded.append(pass_on(z, c, a_send.at[depth, c], z - 1))
+
+    def arrive(step):
+        for c in range(chunks):
+            for g in range(step, min(2 * step, depth - 1) + 1):
+                source = group_z(g)
+                due = jnp.abs(source - z) == step
+
+                @pl.when(due)
+                def _():
+                    remote(
+                        token_region(source, c),
+                        token_region(source, c),
+                        a_send.at[g, c],
+                        a_recv.at[source, c],
+                        (me, partner),
+                    ).wait_recv()
+
+                target = jnp.where(source < z, z + 1, z - 1)
+                ahead = due & (target >= 0) & (target < depth)
+                copy = remote(
+                    token_region(source, c),
+                    token_region(source, c),
+                    a_send.at[g, c],
+                    a_recv.at[source, c],
+                    (target * across + x, t),
+                )
+
+                @pl.when(ahead)
+                def _():
+                    copy.start()
+
+                guarded.append((ahead, copy))
+
     slot_rows = lax.broadcasted_iota(jnp.int32, (cap, row_count), 0).astype(jnp.float32)
 
-    def choose(expert):
-        select = jnp.where(slot_rows == key_row[pl.ds(expert, 1), :], 1.0, 0.0)
-        out_ref[expert] = jnp.dot(
-            select.astype(jnp.bfloat16), normed[...], preferred_element_type=jnp.float32
-        ).astype(jnp.bfloat16)
-
-    for k in range(1, n):
-        there = lax.rem(me + k, n)
-        choose(there)
-        copy = remote(
-            out_ref.at[there],
-            piece.at[k, :, column(t, cols)],
-            a_send.at[k],
-            a_recv.at[k],
-            (there, t),
-        )
-        copy.start()
-        sends.append(copy)
-        arrivals.append(copy)
-    choose(me)
-    own_in = pltpu.make_async_copy(out_ref.at[me], piece.at[0, :, column(t, cols)], own_sem.at[0])
-    own_in.start()
+    def select(g):
+        source = group_z(g)
+        if g > 0:
+            remote(
+                key_rows.at[source], key_rows.at[source], k_send.at[g], k_recv.at[source], (me, partner)
+            ).wait_recv()
+        for d in list(range(1, across)) + [0]:
+            there = z * across + lax.rem(x + d, across)
+            chosen = jnp.where(
+                slot_rows == key_rows[source, pl.ds(there, 1), :], 1.0, 0.0
+            ).astype(jnp.bfloat16)
+            value = jnp.dot(
+                chosen, tokens[source], preferred_element_type=jnp.float32
+            ).astype(jnp.bfloat16)
+            if d == 0:
+                piece[g * across, :, column(t, cols)] = value
+            else:
+                slots_out[g, d - 1] = value
+                copy = remote(
+                    slots_out.at[g, d - 1],
+                    piece.at[g * across + d, :, column(t, cols)],
+                    x_send.at[g, d - 1],
+                    x_recv.at[g, d - 1],
+                    (there, t),
+                )
+                copy.start()
+                sends.append(copy)
 
     def fan_region(f, index):
-        return piece.at[pl.ds(f * fan_blocks, fan_blocks), :, column(index, cols)]
-
-    def fan_out(f):
-        for k in range(f * fan_blocks, (f + 1) * fan_blocks):
-            if k == 0:
-                own_in.wait()
-            else:
-                arrivals[k - 1].wait_recv()
+        return piece.at[f, :, column(index, cols)]
+
+    def fan_out(g, d):
+        f = g * across + d
         region = fan_region(f, t)
-        for d in range(1, chips):
+        if d > 0:
+            remote(
+                region, region, x_send.at[g, d - 1], x_recv.at[g, d - 1], (me, partner)
+            ).wait_recv()
+        for e in range(1, chips):
             copy = remote(
-                region, region, y_send.at[d, f], y_recv.at[d, f], (me, chip_at(d))
+                region, region, y_send.at[e, f], y_recv.at[e, f], (me, chip_at(e))
             )
             copy.start()
             sends.append(copy)
@@ -322,22 +410,23 @@
         copy.start()
         sends.append(copy)
 
-    def relay(f):
-        for d in range(1, chips):
-            source = chip_at(-d)
-            region = fan_region(f, source)
-            remote(
-                region, region, y_send.at[d, f], y_recv.at[d, f], (me, partner)
-            ).wait_recv()
-            copy = remote(region, region, p_send.at[d, f], p_recv.at[d, f], (me, partner))
-            copy.start()
-            sends.append(copy)
+    def relay(g):
+        for f in range(g * across, (g + 1) * across):
+            for d in range(1, chips):
+                source = chip_at(-d)
+                region = fan_region(f, source)
+                remote(
+                    region, region, y_send.at[d, f], y_recv.at[d, f], (me, partner)
+                ).wait_recv()
+                copy = remote(region, region, p_send.at[d, f], p_recv.at[d, f], (me, partner))
+                copy.start()
+                sends.append(copy)
 
     def hid_region(g, index):
         return hid.at[g, :, column(index, ffn_local)]
 
     def up_stage(g):
-        for f in range(g * group_fans, (g + 1) * group_fans):
+        for f in range(g * across, (g + 1) * across):
             for d in range(chips):
                 region = fan_region(f, chip_at(-d) + partner - t)
                 remote(
@@ -349,7 +438,7 @@
         step = min(256, ffn_local)
 
         def tile(j, carry):
-            rows = piece[pl.ds(g * group_blocks, group_blocks)].reshape(group_rows, tp * cols)
+            rows = piece[pl.ds(g * across, across)].reshape(group_rows, tp * cols)
             at = pl.ds(pl.multiple_of(j * step, 128), step)
             gate_val = jnp.dot(rows, gate_w[:, at], preferred_element_type=jnp.float32)
             up_val = jnp.dot(rows, up_w[:, at], preferred_element_type=jnp.float32)
@@ -358,6 +447,8 @@
             return carry
 
         lax.fori_loop(0, ffn_local // step, tile, 0)
+
+    def send_hidden(g):
         region = hid_region(g, t)
         for d in range(1, chips):
             copy = remote(
@@ -379,91 +470,96 @@
             copy.start()
             sends.append(copy)
 
-    returns = []
-
-    def down_stage(g):
+    def down_stage(g, first=False):
         for d in range(chips):
             region = hid_region(g, chip_at(-d) + partner - t)
             remote(
                 region, region, hp_send.at[d, g], hp_recv.at[d, g], (me, partner)
             ).wait_recv()
-        if g == 0:
+        if first:
             weight_copies[2].wait()
         step = min(256, cols)
 
         def tile(j, carry):
             at = pl.ds(pl.multiple_of(j * step, 128), step)
             value = jnp.dot(hid[g], down_w[:, at], preferred_element_type=jnp.float32)
-            eo[pl.ds(g * group_blocks, group_blocks), :, at] = value.astype(
-                jnp.bfloat16
-            ).reshape(group_blocks, cap, step)
+            eo[pl.ds(g * across, across), :, at] = value.astype(jnp.bfloat16).reshape(
+                across, cap, step
+            )
             return carry
 
         lax.fori_loop(0, cols // step, tile, 0)
-        for k in range(g * group_blocks, (g + 1) * group_blocks):
-            if k == 0:
-                copy = pltpu.make_async_copy(eo.at[0], ret_ref.at[me], own_sem.at[1])
-            else:
-                copy = remote(
-                    eo.at[k],
-                    ret_ref.at[me],
-                    r_send.at[k],
-                    r_recv.at[k],
-                    (lax.rem(me + n - k, n), t),
-                )
+        for d in range(across):
+            if g == 0 and d == 0:
+                continue
+            k = g * across + d
+            copy = remote(
+                eo.at[k],
+                ret_ref.at[me],
+                r_send.at[k],
+                r_recv.at[me],
+                (group_z(g) * across + lax.rem(x + across - d, across), t),
+            )
             copy.start()
-            returns.append(copy)
-
-    def fans_of(g):
-        return range(g * group_fans, (g + 1) * group_fans)
-
-    ahead = min(2, groups)
-    for g in range(ahead):
-        for f in fans_of(g):
-            fan_out(f)
-    for g in range(groups):
-        for f in fans_of(g):
-            relay(f)
-        up_stage(g)
-        if g + ahead < groups:
-            for f in fans_of(g + ahead):
-                fan_out(f)
-        if g >= 1:
-            relay_hidden(g - 1)
-            down_stage(g - 1)
-    relay_hidden(groups - 1)
-    down_stage(groups - 1)
+            sends.append(copy)
+
+    last = depth - 1
+    select(0)
+    for d in range(across):
+        fan_out(0, d)
+    for s in range(1, depth):
+        arrive(s)
+        select(s)
+        fan_out(s, 0)
+        relay(s - 1)
+        up_stage(s - 1)
+        if s > 1:
+            send_hidden(s - 1)
+        for d in range(1, across):
+            fan_out(s, d)
+        if s > 2:
+            relay_hidden(s - 2)
+            down_stage(s - 2, s == 3)
+    relay(last)
+    up_stage(last)
+    if last > 0:
+        send_hidden(last)
+    send_hidden(0)
+    if last > 1:
+        relay_hidden(last - 1)
+        down_stage(last - 1, last == 2)
+    if last > 0:
+        relay_hidden(last)
+        down_stage(last, last == 1)
+    relay_hidden(0)
+    down_stage(0, last == 0)
 
     slot_lanes = lax.broadcasted_iota(jnp.int32, (row_count, cap), 1).astype(jnp.float32)
-    for g in range(groups):
-        members = range(g * group_blocks, (g + 1) * group_blocks)
-        for k in members:
-            if k == 0:
-                returns[0].wait()
-            else:
-                there = lax.rem(me + k, n)
-                returns[k].wait_send()
+    for g in range(depth):
+        chosen = []
+        for d in range(across):
+            there = group_z(g) * across + lax.rem(x + d, across)
+            own = g == 0 and d == 0
+            if not own:
+                k = g * across + d
                 remote(
-                    eo.at[k], ret_ref.at[there], r_send.at[k], r_recv.at[k], (there, t)
+                    eo.at[k], ret_ref.at[there], r_send.at[k], r_recv.at[there], (me, partner)
                 ).wait_recv()
-        chosen = []
-        for k in members:
-            there = lax.rem(me + k, n)
             here = lanes == there
             key = jnp.sum(jnp.where(here, key_col[...], 0.0), axis=1, keepdims=True)
             weight = jnp.sum(jnp.where(here, mix_col[...], 0.0), axis=1, keepdims=True)
-            select = jnp.where(slot_lanes == key, 1.0, 0.0).astype(jnp.bfloat16)
-            chosen.append((there, select, weight))
+            slot_of = jnp.where(slot_lanes == key, 1.0, 0.0).astype(jnp.bfloat16)
+            chosen.append((eo.at[0] if own else ret_ref.at[there], slot_of, weight))
         step = min(256, cols)
 
         def combine(j, carry):
             at = pl.ds(pl.multiple_of(j * step, 128), step)
             value = jnp.zeros((row_count, step), jnp.float32) if g == 0 else acc[:, at]
-            for there, select, weight in chosen:
+            for source, slot_of, weight in chosen:
                 value = value + weight * jnp.dot(
-                    select, ret_ref[there, :, at], preferred_element_type=jnp.float32
+                    slot_of, source[:, at], preferred_element_type=jnp.float32
                 )
-            if g == groups - 1:
+            if g == depth - 1:
                 result_ref[:, at] = (resid[:, at].astype(jnp.float32) + value).astype(jnp.bfloat16)
             else:
                 acc[:, at] = value
@@ -472,6 +568,8 @@
         lax.fori_loop(0, cols // step, combine, 0)
     for copy in sends:
         copy.wait_send()
+    for started, copy in guarded:
+        pl.when(started)(copy.wait_send)
 
 
 def whole_layer(blocks, weights):
@@ -481,8 +579,9 @@
     cap = 4 * row_count // n
     chips = tp // 2
     rows = n * cap
-    groups = max(1, min(4, rows // 256))
-    fans = min(n, 2 * groups)
+    across = max(d for d in range(1, n + 1) if n % d == 0 and d * d <= n)
+    depth = n // across
+    chunks = 2
     projection, gate_weight, _, down_weight = weights
     width, ffn_local = gate_weight.shape[1], gate_weight.shape[2]
     ffn = down_weight.shape[1]
@@ -490,44 +589,47 @@
     bf16, f32 = jnp.bfloat16, jnp.float32
     flops = 2 * rows * width * ffn_local * 2 + 2 * rows * ffn * cols
     return pl.pallas_call(
-        functools.partial(expert_kernel, n, tp),
+        functools.partial(expert_kernel, n, tp, across),
         out_shape=jax.ShapeDtypeStruct((row_count, cols), bf16),
         in_specs=[pl.BlockSpec(memory_space=pltpu.VMEM)] * len(blocks)
         + [pl.BlockSpec(memory_space=pl.ANY)] * len(weights),
         out_specs=pl.BlockSpec(memory_space=pltpu.VMEM),
         scratch_shapes=[
-            pltpu.VMEM((n, cap, cols), bf16),
+            pltpu.VMEM((depth, row_count, cols), bf16),
+            pltpu.VMEM((depth, max(1, across - 1), cap, cols), bf16),
             pltpu.VMEM((n, cap, cols), bf16),
             pltpu.VMEM((row_count, wide * tp), bf16),
             pltpu.VMEM(projection.shape, bf16),
             pltpu.VMEM((row_count, cols), f32),
             pltpu.VMEM((row_count, cols), bf16),
-            pltpu.VMEM((row_count, cols), bf16),
             pltpu.VMEM((tp, 8, row_count), f32),
             pltpu.VMEM((row_count, 128), f32),
-            pltpu.VMEM((128, row_count), f32),
+            pltpu.VMEM((depth, -(-n // 8) * 8, row_count), f32),
             pltpu.VMEM((row_count, 128), f32),
             pltpu.VMEM((16, wide), bf16),
             pltpu.VMEM((16, wide), bf16),
             pltpu.VMEM((8, 128), f32),
             pltpu.VMEM((n, cap, width), bf16),
-            pltpu.VMEM((groups, rows // groups, ffn), bf16),
+            pltpu.VMEM((depth, rows // depth, ffn), bf16),
             pltpu.VMEM((n, cap, cols), bf16),
             pltpu.VMEM((width, ffn_local), bf16),
             pltpu.VMEM((width, ffn_local), bf16),
             pltpu.VMEM((ffn, cols), bf16),
             dma((4,)),
-            dma((2,)),
-            dma((n,)),
-            dma((n,)),
-            dma((chips, fans)),
-            dma((chips, fans)),
-            dma((chips, fans)),
-            dma((chips, fans)),
-            dma((chips, groups)),
-            dma((chips, groups)),
-            dma((chips, groups)),
-            dma((chips, groups)),
+            dma((depth,)),
+            dma((depth,)),
+            dma((depth + 1, chunks)),
+            dma((depth, chunks)),
+            dma((depth, across)),
+            dma((depth, across)),
+            dma((chips, n)),
+            dma((chips, n)),
+            dma((chips, n)),
+            dma((chips, n)),
+            dma((chips, depth)),
+            dma((chips, depth)),
+            dma((chips, depth)),
+            dma((chips, depth)),
             dma((n,)),
             dma((n,)),
             dma((3,)),

time: 149 us -> 143 us (0.960)
  Pallas kernels: 141 us -> 135 us
    pallas_call x1, Pallas kernels: 141 us -> 135 us  [whole_layer(): pl.pallas_call(functools.partial(expert_kernel, n, tp, across), out_shape...]
where the time goes in v1:
time: 143 us
  Pallas kernels  135 us (94%)
  local copies, waits for them, and re-layouts  5.5 us (4%)
  other arithmetic  2.14 us (1%)
    pallas_call x1, Pallas kernels, whole_layer(): pl.pallas_call(functools.partial(expert_kernel, n, tp, across), out_shape...  135 us
    unnamed x2, local copies, waits for them, and re-layouts  3.34 us

profile of v1, /device:TPU:0, one launch (start us, length us, event | category | flops | bytes accessed | tf_op | source)
XLA Modules:
  0.0 142.5 jit_solution(15340261364666407892)
XLA Ops:
  0.0 0.7 convert_element_type.3
  0.7 0.7 fusion
  1.4 1.3 broadcast_in_dim.5.gain_ref
  2.7 0.8 broadcast_in_dim.4.docs_ref
  3.4 0.1 copy.18
  3.6 0.8 broadcast_divide_fusion.mix_ref
  4.3 1.5 %copy.20.ids_ref = s32[256,2]{1,0:T(8,128)} copy(s32[256,2]{0,1:T(2,128)} %param.22) | data formatting | bytes 4096 | tf_op args[8]
  5.8 134.9 %layer.1 = bf16[256,1024]{1,0:T(8,128)(2,1)} custom-call(bf16[256,512]{1,0:T(8,128)(2,1)} %outer_ref.1, bf16[256,512]{1,0:T(8,128)(2,1)} %inner_ref.1, bf16[256,512]{1,0:T(8,128)(2,1)} %conv_ref.1, bf16[3,512]{1,0:T(4,128)(2,1)} %taps_ref.1, f32[256,128]{1,0:T(8,128)} %broadcast_in_dim.4.docs_ref, bf16[256,1024]{1,0:T(8,128)(2,1)} %residual_ref.1, ...), custom_call_target="tpu_custom_call" | custom-call | flops 12884901888 | bytes 12582912 | tf_op jit(solution)/shard_map/layer/pallas_call | solution.py:591
  140.7 1.9 %copy.22 = bf16[256,1024]{1,0:T(8,128)(2,1)} copy(bf16[256,1024]{1,0:T(8,128)(2,1)} %layer.1) | data formatting | bytes 1048576

commit v2 on v1

--- a/solution.py
+++ b/solution.py
@@ -34,6 +34,7 @@
     residual_ref,
     gain_ref,
     ids_ref,
+    group_ref,
     mix_ref,
     proj_hbm,
     gate_hbm,
@@ -48,9 +49,13 @@
     acc,
     resid,
     squares,
+    total,
+    scales,
+    gain_row,
     key_col,
     key_rows,
     mix_col,
+    docs_rows,
     halo_inner,
     halo_conv,
     halo_docs,
@@ -63,6 +68,8 @@
     w_sem,
     k_send,
     k_recv,
+    c_send,
+    c_recv,
     a_send,
     a_recv,
     x_send,
@@ -139,12 +146,60 @@
         pl.semaphore_signal(
             barrier, inc=1, device_id=(me, lax.rem(t + d, tp)), device_id_type=MESH
         )
-    pl.semaphore_wait(barrier, n - 1 + tp - 1)
 
     sends = []
-    arrivals = []
     row_count = residual_ref.shape[0]
     wide = branch.shape[1] // tp
+    half = row_count // 2
+
+    experts = lax.broadcasted_iota(jnp.int32, (128, row_count), 0)
+    is_first, is_second = experts == ids_ref[0:1, :], experts == ids_ref[1:2, :]
+    pair = mix_ref[...]
+    mix = group_ref[...].reshape(1, row_count) * pair / (pair[0:1] + pair[1:2])
+    mix_rows = jnp.where(is_first, mix[0:1], 0.0) + jnp.where(is_second, mix[1:2], 0.0)
+    mix_col[...] = mix_rows.T
+    member = jnp.where(is_first, 1.0, 0.0) + jnp.where(is_second, 1.0, 0.0)
+    earlier = jnp.where(
+        lax.broadcasted_iota(jnp.int32, (row_count, row_count), 0)
+        < lax.broadcasted_iota(jnp.int32, (row_count, row_count), 1),
+        1.0,
+        0.0,
+    ).astype(jnp.bfloat16)
+    ranks = jnp.dot(member.astype(jnp.bfloat16), earlier, preferred_element_type=jnp.float32)
+    keys = jnp.where(member > 0.5, ranks, -1.0)
+    key_col[...] = keys.T
+    key_rows[me] = keys[0:key_count]
+    gain_row[...] = gain_ref[...].reshape(1, cols).astype(jnp.float32)
+
+    docs = jnp.broadcast_to(docs_ref[...].reshape(1, row_count).astype(jnp.float32), (8, row_count))
+    docs_rows[...] = docs
+    position = lax.broadcasted_iota(jnp.int32, (8, row_count), 1)
+
+    def as_column(mask):
+        rows = jnp.where(mask, 1.0, 0.0)[0:1]
+        return jnp.broadcast_to(rows, (128, rows.shape[1])).T > 0.5
+
+    same_one = as_column((pltpu.roll(docs, 1, 1) == docs) & (position >= 1))
+    same_two = as_column((pltpu.roll(docs, 2, 1) == docs) & (position >= 2))
+
+    def weigh(at, products, one, two, first, second, outer):
+        taps = taps_ref[:, at].astype(jnp.float32)
+        conv = taps[2:3] * products
+        conv = conv + jnp.where(first, taps[1:2] * one, 0.0)
+        conv = conv + jnp.where(second, taps[0:1] * two, 0.0)
+        return (outer.astype(jnp.float32) * conv).astype(jnp.bfloat16)
+
+    def conv_tile(j, carry):
+        at = pl.ds(pl.multiple_of(j * 128, 128), 128)
+        products = inner_ref[:, at].astype(jnp.float32) * conv_ref[:, at].astype(jnp.float32)
+        one, two = pltpu.roll(products, 1, 0), pltpu.roll(products, 2, 0)
+        value = weigh(at, products, one, two, same_one, same_two, outer_ref[:, at])
+        branch[:, pl.ds(pl.multiple_of(t * wide + j * 128, 128), 128)] = value
+        return carry
+
+    lax.fori_loop(0, wide // 128, conv_tile, 0)
+
+    pl.semaphore_wait(barrier, n - 1 + tp - 1)
 
     halos = []
     following = (lax.rem(me + 1, n), t)
@@ -152,7 +207,7 @@
         (
             (inner_ref.at[pl.ds(row_count - 16, 16)], halo_inner),
             (conv_ref.at[pl.ds(row_count - 16, 16)], halo_conv),
-            (docs_ref.at[pl.ds(row_count - 8, 8)], halo_docs),
+            (docs_rows.at[:, pl.ds(row_count - 128, 128)], halo_docs),
         )
     ):
         copy = remote(source, target, h_send.at[i], h_recv.at[i], following)
@@ -160,85 +215,58 @@
         halos.append(copy)
         sends.append(copy)
 
-    lanes = lax.broadcasted_iota(jnp.int32, (row_count, 128), 1)
-    first_id, second_id = ids_ref[:, 0:1], ids_ref[:, 1:2]
-    is_first, is_second = lanes == first_id, lanes == second_id
-    mix_col[...] = jnp.where(is_first, mix_ref[:, 0:1], 0.0) + jnp.where(
-        is_second, mix_ref[:, 1:2], 0.0
-    )
-    member = jnp.where(is_first, 1.0, 0.0) + jnp.where(is_second, 1.0, 0.0)
-    earlier = jnp.where(
-        lax.broadcasted_iota(jnp.int32, (row_count, row_count), 1)
-        < lax.broadcasted_iota(jnp.int32, (row_count, row_count), 0),
-        1.0,
-        0.0,
-    ).astype(jnp.bfloat16)
-    ranks = jnp.dot(earlier, member.astype(jnp.bfloat16), preferred_element_type=jnp.float32)
-    keys = jnp.where(member > 0.5, ranks, -1.0)
-    key_col[...] = keys
-    key_rows[z] = keys.T[0:key_count]
-    for d in range(1, depth):
+    def branch_region(index, h):
+        return branch.at[pl.ds(h * half, half), column(index, wide)]
+
+    def send_branch(h):
+        region = branch_region(t, h)
+        for d in range(1, chips):
+            copy = remote(region, region, by_send.at[d, h], by_recv.at[d, h], (me, chip_at(d)))
+            copy.start()
+            sends.append(copy)
+        copy = remote(region, region, bp_send.at[0, h], bp_recv.at[0, h], (me, partner))
+        copy.start()
+        sends.append(copy)
+
+    send_branch(1)
+    for d in range(1, n):
         copy = remote(
-            key_rows.at[z],
-            key_rows.at[z],
+            key_rows.at[me],
+            key_rows.at[me],
             k_send.at[d],
-            k_recv.at[z],
-            (lax.rem(z + d, depth) * across + x, t),
+            k_recv.at[me],
+            (lax.rem(me + d, n), t),
         )
         copy.start()
         sends.append(copy)
 
     for copy in halos:
         copy.wait_recv()
-    row_at = lax.broadcasted_iota(jnp.int32, (row_count, 1), 0)
-    own_docs = docs_ref[:, 0:1]
-    halo_ids = jnp.where(me > 0, halo_docs[...], -1.0)[:, 0:1]
-    docs_one = jnp.where(row_at == 0, halo_ids[7:8], pltpu.roll(docs_ref[...], 1, 0)[:, 0:1])
-    docs_two = jnp.where(
-        row_at == 0,
-        halo_ids[6:7],
-        jnp.where(row_at == 1, halo_ids[7:8], pltpu.roll(docs_ref[...], 2, 0)[:, 0:1]),
-    )
-    same_one, same_two = docs_one == own_docs, docs_two == own_docs
-
-    def conv_tile(j, carry):
-        at = pl.ds(pl.multiple_of(j * 128, 128), 128)
-        products = inner_ref[:, at].astype(jnp.float32) * conv_ref[:, at].astype(jnp.float32)
+    lane = lax.broadcasted_iota(jnp.int32, (8, 128), 1)
+    near_docs = docs_rows[:, 0:128]
+    past_docs = jnp.where(me > 0, halo_docs[...], -1.0)
+    docs_one = jnp.where(lane < 1, pltpu.roll(past_docs, 1, 1), pltpu.roll(near_docs, 1, 1))
+    docs_two = jnp.where(lane < 2, pltpu.roll(past_docs, 2, 1), pltpu.roll(near_docs, 2, 1))
+    edge_one = as_column(docs_one == near_docs)[0:16]
+    edge_two = as_column(docs_two == near_docs)[0:16]
+    row_at = lax.broadcasted_iota(jnp.int32, (16, 1), 0)
+    for j in range(wide // 128):
+        at = pl.ds(j * 128, 128)
+        products = inner_ref[0:16, at].astype(jnp.float32) * conv_ref[0:16, at].astype(jnp.float32)
         before = halo_inner[:, at].astype(jnp.float32) * halo_conv[:, at].astype(jnp.float32)
-        one = jnp.where(row_at == 0, before[15:16], pltpu.roll(products, 1, 0))
-        two = jnp.where(
-            row_at == 0,
-            before[14:15],
-            jnp.where(row_at == 1, before[15:16], pltpu.roll(products, 2, 0)),
-        )
-        taps = taps_ref[:, at].astype(jnp.float32)
-        conv = taps[2:3] * products
-        conv = conv + jnp.where(same_one, taps[1:2] * one, 0.0)
-        conv = conv + jnp.where(same_two, taps[0:1] * two, 0.0)
-        value = (outer_ref[:, at].astype(jnp.float32) * conv).astype(jnp.bfloat16)
-        branch[:, pl.ds(pl.multiple_of(t * wide + j * 128, 128), 128)] = value
-        return carry
-
-    lax.fori_loop(0, wide // 128, conv_tile, 0)
-
-    def branch_region(index):
-        return branch.at[:, column(index, wide)]
-
-    region = branch_region(t)
-    for d in range(1, chips):
-        copy = remote(region, region, by_send.at[d], by_recv.at[d], (me, chip_at(d)))
-        copy.start()
-        sends.append(copy)
-    copy = remote(region, region, bp_send.at[0], bp_recv.at[0], (me, partner))
-    copy.start()
-    sends.append(copy)
+        one = jnp.where(row_at < 1, pltpu.roll(before, 1, 0), pltpu.roll(products, 1, 0))
+        two = jnp.where(row_at < 2, pltpu.roll(before, 2, 0), pltpu.roll(products, 2, 0))
+        value = weigh(at, products, one, two, edge_one, edge_two, outer_ref[0:16, at])
+        branch[0:16, pl.ds(pl.multiple_of(t * wide + j * 128, 128), 128)] = value
+    send_branch(0)
     weight_copies[3].wait()
 
-    def project(index, first=False):
-        step = min(256, cols)
-
+    chunk = cols // chunks
+    step_cols = min(256, chunk)
+
+    def project(index, first=False, c=None):
         def tile(j, carry):
-            at = pl.ds(pl.multiple_of(j * step, 128), step)
+            at = pl.ds(pl.multiple_of(j * step_cols, 128), step_cols)
             rows = pl.ds(pl.multiple_of(index * wide, 128), wide)
             value = jnp.dot(
                 branch[:, column(index, wide)], proj_w[rows, at], preferred_element_type=jnp.float32
@@ -246,63 +274,34 @@
             acc[:, at] = value if first else acc[:, at] + value
             return carry
 
-        lax.fori_loop(0, cols // step, tile, 0)
+        tiles = chunk // step_cols
+        lo, hi = (0, chunks * tiles) if c is None else (c * tiles, (c + 1) * tiles)
+        lax.fori_loop(lo, hi, tile, 0)
+
+    def branch_arrived(index, sem, h):
+        region = branch_region(index, h)
+        return remote(region, region, sem, sem, (me, partner))
 
     project(t, True)
-    other = branch_region(partner)
-    remote(other, other, bp_send.at[0], bp_recv.at[0], (me, partner)).wait_recv()
+    for h in (1, 0):
+        branch_arrived(partner, bp_recv.at[0, h], h).wait_recv()
     project(partner)
     for d in range(1, chips):
         source = chip_at(-d)
-        region = branch_region(source)
-        remote(region, region, by_send.at[d], by_recv.at[d], (me, partner)).wait_recv()
-        copy = remote(region, region, bp_send.at[d], bp_recv.at[d], (me, partner))
-        copy.start()
-        sends.append(copy)
+        for h in (1, 0):
+            branch_arrived(source, by_recv.at[d, h], h).wait_recv()
+            region = branch_region(source, h)
+            copy = remote(region, region, bp_send.at[d, h], bp_recv.at[d, h], (me, partner))
+            copy.start()
+            sends.append(copy)
         project(source)
     for d in range(1, chips):
         source = chip_at(-d) + partner - t
-        region = branch_region(source)
-        remote(region, region, bp_send.at[d], bp_recv.at[d], (me, partner)).wait_recv()
-        project(source)
-
-    def resid_tile(j, total):
-        at = pl.ds(pl.multiple_of(j * 128, 128), 128)
-        value = (residual_ref[:, at].astype(jnp.float32) + acc[:, at]).astype(jnp.bfloat16)
-        resid[:, at] = value
-        value = value.astype(jnp.float32)
-        return total + value * value
-
-    total = lax.fori_loop(
-        0, cols // 128, resid_tile, jnp.zeros((row_count, 128), jnp.float32)
-    )
-    squares[t] = jnp.broadcast_to(
-        jnp.sum(total.T, axis=0, keepdims=True), (8, row_count)
-    )
-    for d in range(1, tp):
-        copy = remote(
-            squares.at[t], squares.at[t], s_send.at[d], s_recv.at[d], (me, lax.rem(t + d, tp))
-        )
-        copy.start()
-        sends.append(copy)
-    for d in range(1, tp):
-        source = lax.rem(t + tp - d, tp)
-        remote(
-            squares.at[source], squares.at[source], s_send.at[d], s_recv.at[d], (me, source)
-        ).wait_recv()
-    total_sq = jnp.sum(squares[...], axis=0)[0:1]
-    scale_row = lax.rsqrt(total_sq / (tp * cols) + EPS)
-    scale = jnp.broadcast_to(scale_row, (128, row_count)).T
-
-    def norm_tile(j, carry):
-        at = pl.ds(pl.multiple_of(j * 128, 128), 128)
-        value = resid[:, at].astype(jnp.float32) * scale * gain_ref[:, at].astype(jnp.float32)
-        tokens[z, :, at] = value.astype(jnp.bfloat16)
-        return carry
-
-    lax.fori_loop(0, cols // 128, norm_tile, 0)
-
-    chunk = cols // chunks
+        for h in (1, 0):
+            branch_arrived(source, bp_recv.at[d, h], h).wait_recv()
+        if d < chips - 1:
+            project(source)
+
     guarded = []
 
     def token_region(index, c):
@@ -324,9 +323,51 @@
 
         return inside, copy
 
+    total[...] = jnp.zeros_like(total)
+
+    def resid_tile(j, carry):
+        at = pl.ds(pl.multiple_of(j * 128, 128), 128)
+        value = (residual_ref[:, at].astype(jnp.float32) + acc[:, at]).astype(jnp.bfloat16)
+        resid[:, at] = value
+        value = value.astype(jnp.float32)
+        total[...] += value * value
+        tokens[z, :, at] = (value * gain_row[:, at]).astype(jnp.bfloat16)
+        return carry
+
     for c in range(chunks):
+        if chips > 1:
+            project(source, c=c)
+        lax.fori_loop(c * chunk // 128, (c + 1) * chunk // 128, resid_tile, 0)
         guarded.append(pass_on(z, c, a_send.at[0, c], z + 1))
         guarded.append(pass_on(z, c, a_send.at[depth, c], z - 1))
+    squares[t] = jnp.broadcast_to(
+        jnp.sum(total[...].T, axis=0, keepdims=True), (8, row_count)
+    )
+    for d in range(1, tp):
+        copy = remote(
+            squares.at[t], squares.at[t], s_send.at[d], s_recv.at[d], (me, lax.rem(t + d, tp))
+        )
+        copy.start()
+        sends.append(copy)
+
+    def share_scale():
+        for d in range(1, tp):
+            other = lax.rem(t + tp - d, tp)
+            remote(
+                squares.at[other], squares.at[other], s_send.at[d], s_recv.at[d], (me, other)
+            ).wait_recv()
+        total_sq = jnp.sum(squares[...], axis=0)
+        scales[me] = lax.rsqrt(total_sq / (tp * cols) + EPS)
+        for d in range(1, n):
+            copy = remote(
+                scales.at[me],
+                scales.at[me],
+                c_send.at[d],
+                c_recv.at[me],
+                (lax.rem(me + d, n), t),
+            )
+            copy.start()
+            sends.append(copy)
 
     def arrive(step):
         for c in range(chunks):
@@ -362,16 +403,31 @@
 
     slot_rows = lax.broadcasted_iota(jnp.int32, (cap, row_count), 0).astype(jnp.float32)
 
+    def wait_keys(origin):
+        remote(
+            key_rows.at[origin], key_rows.at[origin], k_send.at[1], k_recv.at[origin], (me, partner)
+        ).wait_recv()
+
+    def slot_scale(g, d):
+        origin = group_z(g) * across + lax.rem(x + across - d, across)
+        if d > 0:
+            wait_keys(origin)
+        if g > 0 or d > 0:
+            remote(
+                scales.at[origin], scales.at[origin], c_send.at[1], c_recv.at[origin], (me, partner)
+            ).wait_recv()
+        mine = slot_rows == key_rows[origin, pl.ds(me, 1), :]
+        return jnp.sum(jnp.where(mine, scales[origin, 0:1, :], 0.0), axis=1, keepdims=True)
+
     def select(g):
         source = group_z(g)
+        origin = source * across + x
         if g > 0:
-            remote(
-                key_rows.at[source], key_rows.at[source], k_send.at[g], k_recv.at[source], (me, partner)
-            ).wait_recv()
+            wait_keys(origin)
         for d in list(range(1, across)) + [0]:
             there = z * across + lax.rem(x + d, across)
             chosen = jnp.where(
-                slot_rows == key_rows[source, pl.ds(there, 1), :], 1.0, 0.0
+                slot_rows == key_rows[origin, pl.ds(there, 1), :], 1.0, 0.0
             ).astype(jnp.bfloat16)
             value = jnp.dot(
                 chosen, tokens[source], preferred_element_type=jnp.float32
@@ -435,6 +491,7 @@
         if g == 0:
             weight_copies[0].wait()
             weight_copies[1].wait()
+        scale = jnp.concatenate([slot_scale(g, d) for d in range(across)], axis=0)
         step = min(256, ffn_local)
 
         def tile(j, carry):
@@ -442,7 +499,7 @@
             at = pl.ds(pl.multiple_of(j * step, 128), step)
             gate_val = jnp.dot(rows, gate_w[:, at], preferred_element_type=jnp.float32)
             up_val = jnp.dot(rows, up_w[:, at], preferred_element_type=jnp.float32)
-            hidden = (jax.nn.silu(gate_val) * up_val).astype(jnp.bfloat16)
+            hidden = (jax.nn.silu(gate_val * scale) * (up_val * scale)).astype(jnp.bfloat16)
             hid[g, :, pl.ds(pl.multiple_of(t * ffn_local + j * step, 128), step)] = hidden
             return carry
 
@@ -505,7 +562,9 @@
 
     last = depth - 1
     select(0)
-    for d in range(across):
+    fan_out(0, 0)
+    share_scale()
+    for d in range(1, across):
         fan_out(0, d)
     for s in range(1, depth):
         arrive(s)
@@ -534,6 +593,7 @@
     relay_hidden(0)
     down_stage(0, last == 0)
 
+    lanes = lax.broadcasted_iota(jnp.int32, (row_count, 128), 1)
     slot_lanes = lax.broadcasted_iota(jnp.int32, (row_count, cap), 1).astype(jnp.float32)
     for g in range(depth):
         chosen = []
@@ -604,8 +664,12 @@
             pltpu.VMEM((row_count, cols), bf16),
             pltpu.VMEM((tp, 8, row_count), f32),
             pltpu.VMEM((row_count, 128), f32),
-            pltpu.VMEM((depth, -(-n // 8) * 8, row_count), f32),
+            pltpu.VMEM((n, 8, row_count), f32),
+            pltpu.VMEM((1, cols), f32),
             pltpu.VMEM((row_count, 128), f32),
+            pltpu.VMEM((n, -(-n // 8) * 8, row_count), f32),
+            pltpu.VMEM((row_count, 128), f32),
+            pltpu.VMEM((8, row_count), f32),
             pltpu.VMEM((16, wide), bf16),
             pltpu.VMEM((16, wide), bf16),
             pltpu.VMEM((8, 128), f32),
@@ -616,8 +680,10 @@
             pltpu.VMEM((width, ffn_local), bf16),
             pltpu.VMEM((ffn, cols), bf16),
             dma((4,)),
-            dma((depth,)),
-            dma((depth,)),
+            dma((n,)),
+            dma((n,)),
+            dma((n,)),
+            dma((n,)),
             dma((depth + 1, chunks)),
             dma((depth, chunks)),
             dma((depth, across)),
@@ -634,10 +700,10 @@
             dma((n,)),
             dma((3,)),
             dma((3,)),
-            dma((chips,)),
-            dma((chips,)),
-            dma((chips,)),
-            dma((chips,)),
+            dma((chips, 2)),
+            dma((chips, 2)),
+            dma((chips, 2)),
+            dma((chips, 2)),
             dma((tp,)),
             dma((tp,)),
         ],
@@ -667,22 +733,18 @@
     up_weight,
     down_weight,
 ):
-    row_count = conv_input.shape[0]
-    docs = jnp.broadcast_to(doc_ids.astype(jnp.float32)[:, None], (row_count, 128))
-    mix_weight = (
-        group_weight[:, None] * expert_weight / jnp.sum(expert_weight, axis=1, keepdims=True)
-    )
     return whole_layer(
         (
             outer_gate,
             inner_gate,
             conv_input,
             conv_weight,
-            docs,
+            doc_ids,
             residual,
-            norm_gain[None, :],
-            expert_ids,
-            mix_weight,
+            norm_gain,
+            expert_ids.T,
+            group_weight,
+            expert_weight.T,
         ),
         (output_weight, gate_weight, up_weight, down_weight),
     )

time: 143 us -> 131 us (0.916)
  Pallas kernels: 135 us -> 129 us
  local copies, waits for them, and re-layouts: 5.5 us -> 1.87 us
  other arithmetic: 2.14 us -> 0 us
    pallas_call x1, Pallas kernels: 135 us -> 129 us  [whole_layer(): pl.pallas_call(functools.partial(expert_kernel, n, tp, across), out_shape...]
    broadcast_in_dim x2 -> x0, local copies, waits for them, and re-layouts: 2.03 us -> none  [the longest x1 1.27 us: per_device(): norm_gain[None, :]]
    unnamed x2 -> x1, local copies, waits for them, and re-layouts: 3.34 us -> 1.87 us
where the time goes in v2:
time: 131 us; the launch traced here: 130 us
  Pallas kernels  129 us (98%)
  local copies, waits for them, and re-layouts  1.87 us (1%)
    pallas_call x1, Pallas kernels, whole_layer(): pl.pallas_call(functools.partial(expert_kernel, n, tp, across), out_shape...  129 us

profile of v2, /device:TPU:0, one launch (start us, length us, event | category | flops | bytes accessed | tf_op | source)
XLA Modules:
  0.0 130.5 jit_solution(1215827153830981133)
XLA Ops:
  0.0 128.6 %layer.1 = bf16[256,1024]{1,0:T(8,128)(2,1)} custom-call(bf16[256,512]{1,0:T(8,128)(2,1)} %outer_ref.1, bf16[256,512]{1,0:T(8,128)(2,1)} %inner_ref.1, bf16[256,512]{1,0:T(8,128)(2,1)} %conv_ref.1, bf16[3,512]{1,0:T(4,128)(2,1)} %taps_ref.1, s32[256]{0:T(256)} %docs_ref.1, bf16[256,1024]{1,0:T(8,128)(2,1)} %residual_ref.1, bf16[1024]{0:T(1024)(128)(2,1)} %gain_ref.1, ...), custom_call_target="tpu_custom_call" | custom-call | flops 12884901888 | bytes 12582912 | tf_op jit(solution)/shard_map/layer/pallas_call | solution.py:651
  128.6 1.9 %copy.16 = bf16[256,1024]{1,0:T(8,128)(2,1)} copy(bf16[256,1024]{1,0:T(8,128)(2,1)} %layer.1) | data formatting | bytes 1048576

commit v3 on v2

--- a/solution.py
+++ b/solution.py
@@ -42,6 +42,7 @@
     down_hbm,
     result_ref,
     tokens,
+    early,
     slots_out,
     ret_ref,
     branch,
@@ -70,6 +71,8 @@
     k_recv,
     c_send,
     c_recv,
+    e_send,
+    e_recv,
     a_send,
     a_recv,
     x_send,
@@ -102,7 +105,10 @@
     ffn_local = gate_w.shape[1]
     depth, group_rows = hid.shape[0], hid.shape[1]
     z, x = lax.div(me, across), lax.rem(me, across)
-    chunks = a_recv.shape[1]
+    ahead_cols = early.shape[2] if e_send.shape[0] > 1 else 0
+    chunks = x_recv.shape[2] - 1
+    last = depth - 1
+    pieces = chunks + (1 if ahead_cols else 0)
     key_count = key_rows.shape[1]
 
     near = jnp.minimum(z, depth - 1 - z)
@@ -114,8 +120,10 @@
         step = (g + 1) // 2
         outward = step if g % 2 else -step
         close = jnp.where(low, z + outward, z - outward)
-        far = jnp.where(low, g, depth - 1 - g)
-        return jnp.where(g <= 2 * near, close, far)
+        return jnp.where(g <= 2 * near, close, jnp.where(low, g, depth - 1 - g))
+
+    def is_early(g):
+        return jnp.abs(group_z(g) - z) < g
 
     def column(index, width):
         return pl.ds(pl.multiple_of(index * width, 128), width)
@@ -262,6 +270,7 @@
     weight_copies[3].wait()
 
     chunk = cols // chunks
+    hid_step = ffn_local // hy_send.shape[2]
     step_cols = min(256, chunk)
 
     def project(index, first=False, c=None):
@@ -305,6 +314,8 @@
     guarded = []
 
     def token_region(index, c):
+        if c == chunks:
+            return early.at[index]
         return tokens.at[index, :, pl.ds(c * chunk, chunk)]
 
     def pass_on(index, c, sem, target):
@@ -322,33 +333,6 @@
             copy.start()
 
         return inside, copy
-
-    total[...] = jnp.zeros_like(total)
-
-    def resid_tile(j, carry):
-        at = pl.ds(pl.multiple_of(j * 128, 128), 128)
-        value = (residual_ref[:, at].astype(jnp.float32) + acc[:, at]).astype(jnp.bfloat16)
-        resid[:, at] = value
-        value = value.astype(jnp.float32)
-        total[...] += value * value
-        tokens[z, :, at] = (value * gain_row[:, at]).astype(jnp.bfloat16)
-        return carry
-
-    for c in range(chunks):
-        if chips > 1:
-            project(source, c=c)
-        lax.fori_loop(c * chunk // 128, (c + 1) * chunk // 128, resid_tile, 0)
-        guarded.append(pass_on(z, c, a_send.at[0, c], z + 1))
-        guarded.append(pass_on(z, c, a_send.at[depth, c], z - 1))
-    squares[t] = jnp.broadcast_to(
-        jnp.sum(total[...].T, axis=0, keepdims=True), (8, row_count)
-    )
-    for d in range(1, tp):
-        copy = remote(
-            squares.at[t], squares.at[t], s_send.at[d], s_recv.at[d], (me, lax.rem(t + d, tp))
-        )
-        copy.start()
-        sends.append(copy)
 
     def share_scale():
         for d in range(1, tp):
@@ -369,38 +353,6 @@
             copy.start()
             sends.append(copy)
 
-    def arrive(step):
-        for c in range(chunks):
-            for g in range(step, min(2 * step, depth - 1) + 1):
-                source = group_z(g)
-                due = jnp.abs(source - z) == step
-
-                @pl.when(due)
-                def _():
-                    remote(
-                        token_region(source, c),
-                        token_region(source, c),
-                        a_send.at[g, c],
-                        a_recv.at[source, c],
-                        (me, partner),
-                    ).wait_recv()
-
-                target = jnp.where(source < z, z + 1, z - 1)
-                ahead = due & (target >= 0) & (target < depth)
-                copy = remote(
-                    token_region(source, c),
-                    token_region(source, c),
-                    a_send.at[g, c],
-                    a_recv.at[source, c],
-                    (target * across + x, t),
-                )
-
-                @pl.when(ahead)
-                def _():
-                    copy.start()
-
-                guarded.append((ahead, copy))
-
     slot_rows = lax.broadcasted_iota(jnp.int32, (cap, row_count), 0).astype(jnp.float32)
 
     def wait_keys(origin):
@@ -419,122 +371,214 @@
         mine = slot_rows == key_rows[origin, pl.ds(me, 1), :]
         return jnp.sum(jnp.where(mine, scales[origin, 0:1, :], 0.0), axis=1, keepdims=True)
 
-    def select(g):
+    def fan_region(f, index, c, late=False):
+        lo = max(c * chunk, ahead_cols) if late else c * chunk
+        hi = (c + 1) * chunk
+        if c == chunks:
+            lo, hi = 0, ahead_cols
+        return piece.at[f, :, pl.ds(pl.multiple_of(index * cols + lo, 128), hi - lo)]
+
+    def home(c):
+        return chip_at(1) if c == chunks else t
+
+    def select(g, c, far=True):
         source = group_z(g)
         origin = source * across + x
-        if g > 0:
-            wait_keys(origin)
-        for d in list(range(1, across)) + [0]:
-            there = z * across + lax.rem(x + d, across)
-            chosen = jnp.where(
-                slot_rows == key_rows[origin, pl.ds(there, 1), :], 1.0, 0.0
-            ).astype(jnp.bfloat16)
-            value = jnp.dot(
-                chosen, tokens[source], preferred_element_type=jnp.float32
-            ).astype(jnp.bfloat16)
-            if d == 0:
-                piece[g * across, :, column(t, cols)] = value
-            else:
-                slots_out[g, d - 1] = value
-                copy = remote(
-                    slots_out.at[g, d - 1],
-                    piece.at[g * across + d, :, column(t, cols)],
-                    x_send.at[g, d - 1],
-                    x_recv.at[g, d - 1],
-                    (there, t),
-                )
-                copy.start()
-                sends.append(copy)
-
-    def fan_region(f, index):
-        return piece.at[f, :, column(index, cols)]
-
-    def fan_out(g, d):
+        peers = [z * across + lax.rem(x + d, across) for d in range(across)]
+        at = pl.ds(0, ahead_cols) if c == chunks else pl.ds(c * chunk, chunk)
+        buffer = early if c == chunks else tokens
+        lo = cols if c == chunks else c * chunk
+        width = ahead_cols if c == chunks else chunk
+        slots = [
+            slots_out.at[g, d - 1, :, pl.ds(lo, width)] for d in range(1, across)
+        ]
+        crossing = [
+            remote(
+                slots[d - 1],
+                fan_region(g * across + d, home(c), c),
+                x_send.at[g, d - 1, c],
+                x_recv.at[g, d - 1, c],
+                (peers[d], t),
+            )
+            for d in range(1, across)
+        ]
+        staying = fan_copies(g, 0, c)
+        if far:
+            sends.extend(crossing + staying)
+
+        def body():
+            if g > 0 and c == 0:
+                wait_keys(origin)
+            for d in list(range(1, across)) + [0]:
+                chosen = jnp.where(
+                    slot_rows == key_rows[origin, pl.ds(peers[d], 1), :], 1.0, 0.0
+                ).astype(jnp.bfloat16)
+                value = jnp.dot(
+                    chosen, buffer[source, :, at], preferred_element_type=jnp.float32
+                ).astype(jnp.bfloat16)
+                if d == 0:
+                    fan_region(g * across, home(c), c)[...] = value
+                    for copy in staying if far else ():
+                        copy.start()
+                else:
+                    slots[d - 1][...] = value
+                    crossing[d - 1].start()
+
+        return body
+
+    def fan_copies(g, d, c):
         f = g * across + d
-        region = fan_region(f, t)
-        if d > 0:
-            remote(
-                region, region, x_send.at[g, d - 1], x_recv.at[g, d - 1], (me, partner)
-            ).wait_recv()
-        for e in range(1, chips):
-            copy = remote(
-                region, region, y_send.at[e, f], y_recv.at[e, f], (me, chip_at(e))
-            )
+        region = fan_region(f, home(c), c)
+        late = fan_region(f, t, c, True)
+        copies = [
+            remote(late, late, y_send.at[e, f, c], y_recv.at[e, f, c], (me, chip_at(e)))
+            for e in range(1, chips if c < chunks else 1)
+        ]
+        copies.append(
+            remote(region, region, p_send.at[0, f, c], p_recv.at[0, f, c], (me, partner))
+        )
+        return copies
+
+    def fan_out(g, d, c):
+        region = fan_region(g * across + d, home(c), c)
+        remote(
+            region, region, x_send.at[g, d - 1, c], x_recv.at[g, d - 1, c], (me, partner)
+        ).wait_recv()
+        for copy in fan_copies(g, d, c):
             copy.start()
             sends.append(copy)
-        copy = remote(region, region, p_send.at[0, f], p_recv.at[0, f], (me, partner))
-        copy.start()
-        sends.append(copy)
+
+    def arrive(step, c):
+        for g in range(step, min(2 * step, depth - 1) + 1):
+            source = group_z(g)
+            due = jnp.abs(source - z) == step
+
+            @pl.when(due)
+            def _():
+                remote(
+                    token_region(source, c),
+                    token_region(source, c),
+                    a_send.at[g, c],
+                    a_recv.at[source, c],
+                    (me, partner),
+                ).wait_recv()
+
+            target = jnp.where(source < z, z + 1, z - 1)
+            ahead = due & (target >= 0) & (target < depth)
+            copy = remote(
+                token_region(source, c),
+                token_region(source, c),
+                a_send.at[g, c],
+                a_recv.at[source, c],
+                (target * across + x, t),
+            )
+
+            @pl.when(ahead)
+            def _():
+                copy.start()
+
+            guarded.append((ahead, copy))
+        if step > 1:
+            pl.when(jnp.logical_not(is_early(step)))(select(step, c))
+        else:
+            select(step, c)()
+
+    def select_early(g):
+        if 1 < g < depth:
+            for c in range(pieces):
+                pl.when(is_early(g))(select(g, c, False))
+
+    def release(g):
+        for c in range(pieces if 1 < g < depth else 0):
+            for copy in fan_copies(g, 0, c):
+                pl.when(is_early(g))(copy.start)
 
     def relay(g):
         for f in range(g * across, (g + 1) * across):
-            for d in range(1, chips):
-                source = chip_at(-d)
-                region = fan_region(f, source)
+            for c in range(chunks):
+                for d in range(1, chips):
+                    region = fan_region(f, chip_at(-d), c, True)
+                    remote(
+                        region, region, y_send.at[d, f, c], y_recv.at[d, f, c], (me, partner)
+                    ).wait_recv()
+                    copy = remote(
+                        region, region, p_send.at[d, f, c], p_recv.at[d, f, c], (me, partner)
+                    )
+                    copy.start()
+                    sends.append(copy)
+
+    def hid_region(g, index, h):
+        return hid.at[
+            g, :, pl.ds(pl.multiple_of(index * ffn_local + h * hid_step, 128), hid_step)
+        ]
+
+    def up_stage(g, send=True):
+        for f in range(g * across, (g + 1) * across):
+            for c in range(chunks):
+                for d in range(chips):
+                    region = fan_region(f, chip_at(-d) + partner - t, c, d > 0)
+                    remote(
+                        region, region, p_send.at[d, f, c], p_recv.at[d, f, c], (me, partner)
+                    ).wait_recv()
+            if ahead_cols:
+                region = fan_region(f, chip_at(1) + partner - t, chunks)
                 remote(
-                    region, region, y_send.at[d, f], y_recv.at[d, f], (me, partner)
-                ).wait_recv()
-                copy = remote(region, region, p_send.at[d, f], p_recv.at[d, f], (me, partner))
-                copy.start()
-                sends.append(copy)
-
-    def hid_region(g, index):
-        return hid.at[g, :, column(index, ffn_local)]
-
-    def up_stage(g):
-        for f in range(g * across, (g + 1) * across):
-            for d in range(chips):
-                region = fan_region(f, chip_at(-d) + partner - t)
-                remote(
-                    region, region, p_send.at[d, f], p_recv.at[d, f], (me, partner)
+                    region, region, p_send.at[0, f, chunks], p_recv.at[0, f, chunks], (me, partner)
                 ).wait_recv()
         if g == 0:
             weight_copies[0].wait()
             weight_copies[1].wait()
         scale = jnp.concatenate([slot_scale(g, d) for d in range(across)], axis=0)
-        step = min(256, ffn_local)
-
-        def tile(j, carry):
+
+        for h in range(ffn_local // hid_step):
             rows = piece[pl.ds(g * across, across)].reshape(group_rows, tp * cols)
-            at = pl.ds(pl.multiple_of(j * step, 128), step)
+            at = pl.ds(h * hid_step, hid_step)
             gate_val = jnp.dot(rows, gate_w[:, at], preferred_element_type=jnp.float32)
             up_val = jnp.dot(rows, up_w[:, at], preferred_element_type=jnp.float32)
             hidden = (jax.nn.silu(gate_val * scale) * (up_val * scale)).astype(jnp.bfloat16)
-            hid[g, :, pl.ds(pl.multiple_of(t * ffn_local + j * step, 128), step)] = hidden
-            return carry
-
-        lax.fori_loop(0, ffn_local // step, tile, 0)
-
-    def send_hidden(g):
-        region = hid_region(g, t)
+            hid[
+                g, :, pl.ds(pl.multiple_of(t * ffn_local + h * hid_step, 128), hid_step)
+            ] = hidden
+            if send:
+                send_hidden(g, h)
+
+    def send_hidden(g, h):
+        region = hid_region(g, t, h)
         for d in range(1, chips):
             copy = remote(
-                region, region, hy_send.at[d, g], hy_recv.at[d, g], (me, chip_at(d))
+                region, region, hy_send.at[d, g, h], hy_recv.at[d, g, h], (me, chip_at(d))
             )
             copy.start()
             sends.append(copy)
-        copy = remote(region, region, hp_send.at[0, g], hp_recv.at[0, g], (me, partner))
+        copy = remote(region, region, hp_send.at[0, g, h], hp_recv.at[0, g, h], (me, partner))
         copy.start()
         sends.append(copy)
 
     def relay_hidden(g):
-        for d in range(1, chips):
-            region = hid_region(g, chip_at(-d))
-            remote(
-                region, region, hy_send.at[d, g], hy_recv.at[d, g], (me, partner)
-            ).wait_recv()
-            copy = remote(region, region, hp_send.at[d, g], hp_recv.at[d, g], (me, partner))
-            copy.start()
-            sends.append(copy)
-
-    def down_stage(g, first=False):
-        for d in range(chips):
-            region = hid_region(g, chip_at(-d) + partner - t)
-            remote(
-                region, region, hp_send.at[d, g], hp_recv.at[d, g], (me, partner)
-            ).wait_recv()
-        if first:
+        for h in range(ffn_local // hid_step):
+            for d in range(1, chips):
+                region = hid_region(g, chip_at(-d), h)
+                remote(
+                    region, region, hy_send.at[d, g, h], hy_recv.at[d, g, h], (me, partner)
+                ).wait_recv()
+                copy = remote(
+                    region, region, hp_send.at[d, g, h], hp_recv.at[d, g, h], (me, partner)
+                )
+                copy.start()
+                sends.append(copy)
+
+    down_ready = []
+
+    def down_stage(g):
+        for h in range(ffn_local // hid_step):
+            for d in range(chips):
+                region = hid_region(g, chip_at(-d) + partner - t, h)
+                remote(
+                    region, region, hp_send.at[d, g, h], hp_recv.at[d, g, h], (me, partner)
+                ).wait_recv()
+        if not down_ready:
             weight_copies[2].wait()
+            down_ready.append(g)
         step = min(256, cols)
 
         def tile(j, carry):
@@ -546,7 +590,9 @@
             return carry
 
         lax.fori_loop(0, cols // step, tile, 0)
-        for d in range(across):
+
+    def send_back(g, offsets):
+        for d in offsets:
             if g == 0 and d == 0:
                 continue
             k = g * across + d
@@ -560,42 +606,116 @@
             copy.start()
             sends.append(copy)
 
-    last = depth - 1
-    select(0)
-    fan_out(0, 0)
+    total[...] = jnp.zeros_like(total)
+
+    def resid_tile(j, carry):
+        at = pl.ds(pl.multiple_of(j * 128, 128), 128)
+        value = (residual_ref[:, at].astype(jnp.float32) + acc[:, at]).astype(jnp.bfloat16)
+        resid[:, at] = value
+        value = value.astype(jnp.float32)
+        total[...] += value * value
+        tokens[z, :, at] = (value * gain_row[:, at]).astype(jnp.bfloat16)
+        return carry
+
+    early_copy = None
+    for c in range(chunks):
+        project(source, c=c)
+        lax.fori_loop(c * chunk // 128, (c + 1) * chunk // 128, resid_tile, 0)
+        if c == 0 and ahead_cols:
+            early_copy = remote(
+                tokens.at[z, :, pl.ds(0, ahead_cols)],
+                early.at[z],
+                e_send.at[0],
+                e_recv.at[0],
+                (me, chip_at(1)),
+            )
+            early_copy.start()
+            sends.append(early_copy)
+        guarded.append(pass_on(z, c, a_send.at[0, c], z + 1))
+        guarded.append(pass_on(z, c, a_send.at[depth, c], z - 1))
+        if c == chunks - 1:
+            squares[t] = jnp.broadcast_to(
+                jnp.sum(total[...].T, axis=0, keepdims=True), (8, row_count)
+            )
+            for d in range(1, tp):
+                copy = remote(
+                    squares.at[t],
+                    squares.at[t],
+                    s_send.at[d],
+                    s_recv.at[d],
+                    (me, lax.rem(t + d, tp)),
+                )
+                copy.start()
+                sends.append(copy)
+        select(0, c)()
+    if ahead_cols:
+        early_copy.wait_recv()
+        guarded.append(pass_on(z, chunks, a_send.at[0, chunks], z + 1))
+        guarded.append(pass_on(z, chunks, a_send.at[depth, chunks], z - 1))
+        select(0, chunks)()
+
+    def fan_across(g, c):
+        for d in range(1, across):
+            fan_out(g, d, c)
+
+    for c in range(chunks):
+        fan_across(0, c)
     share_scale()
-    for d in range(1, across):
-        fan_out(0, d)
+
+    def up_part(g, send=True):
+        relay(g)
+        up_stage(g, send)
+
+    def down_part(g, offsets=None):
+        relay_hidden(g)
+        down_stage(g)
+        send_back(g, range(across) if offsets is None else offsets)
+
     for s in range(1, depth):
-        arrive(s)
-        select(s)
-        fan_out(s, 0)
-        relay(s - 1)
-        up_stage(s - 1)
-        if s > 1:
-            send_hidden(s - 1)
-        for d in range(1, across):
-            fan_out(s, d)
-        if s > 2:
-            relay_hidden(s - 2)
-            down_stage(s - 2, s == 3)
-    relay(last)
-    up_stage(last)
+        arrive(s, 0)
+        if s == 1:
+            for c in range(chunks, pieces):
+                fan_across(0, c)
+            for c in range(1, pieces):
+                arrive(s, c)
+            select_early(s + 1)
+            for c in range(pieces):
+                fan_across(s, c)
+            release(s + 1)
+            up_part(0, False)
+        elif s == 2:
+            up_part(s - 1)
+            for c in range(1, pieces):
+                arrive(s, c)
+            select_early(s + 1)
+            for c in range(pieces):
+                fan_across(s, c)
+            release(s + 1)
+        else:
+            down_part(s - 2, [0])
+            for c in range(1, chunks):
+                arrive(s, c)
+            up_part(s - 1)
+            for c in range(chunks, pieces):
+                arrive(s, c)
+            send_back(s - 2, range(1, across))
+            select_early(s + 1)
+            for c in range(pieces):
+                fan_across(s, c)
+            release(s + 1)
+    if last > 1:
+        down_part(last - 1)
+    up_part(last, last > 0)
+    for h in range(ffn_local // hid_step):
+        send_hidden(0, h)
     if last > 0:
-        send_hidden(last)
-    send_hidden(0)
-    if last > 1:
-        relay_hidden(last - 1)
-        down_stage(last - 1, last == 2)
-    if last > 0:
-        relay_hidden(last)
-        down_stage(last, last == 1)
-    relay_hidden(0)
-    down_stage(0, last == 0)
+        down_part(last)
+    down_part(0)
 
     lanes = lax.broadcasted_iota(jnp.int32, (row_count, 128), 1)
     slot_lanes = lax.broadcasted_iota(jnp.int32, (row_count, cap), 1).astype(jnp.float32)
-    for g in range(depth):
+    turns = [*range(1, last), 0, last] if last > 0 else [0]
+    for turn, g in enumerate(turns):
         chosen = []
         for d in range(across):
             there = group_z(g) * across + lax.rem(x + d, across)
@@ -614,12 +734,12 @@
 
         def combine(j, carry):
             at = pl.ds(pl.multiple_of(j * step, 128), step)
-            value = jnp.zeros((row_count, step), jnp.float32) if g == 0 else acc[:, at]
+            value = jnp.zeros((row_count, step), jnp.float32) if turn == 0 else acc[:, at]
             for source, slot_of, weight in chosen:
                 value = value + weight * jnp.dot(
                     slot_of, source[:, at], preferred_element_type=jnp.float32
                 )
-            if g == depth - 1:
+            if turn == depth - 1:
                 result_ref[:, at] = (resid[:, at].astype(jnp.float32) + value).astype(jnp.bfloat16)
             else:
                 acc[:, at] = value
@@ -641,12 +761,14 @@
     rows = n * cap
     across = max(d for d in range(1, n + 1) if n % d == 0 and d * d <= n)
     depth = n // across
-    chunks = 2
+    chunks = 2 if chips == 2 else 1
+    ahead_cols = cols // 4 if chips == 2 else 0
     projection, gate_weight, _, down_weight = weights
     width, ffn_local = gate_weight.shape[1], gate_weight.shape[2]
     ffn = down_weight.shape[1]
     dma = pltpu.SemaphoreType.DMA
     bf16, f32 = jnp.bfloat16, jnp.float32
+    parts = max(1, ffn_local // 256)
     flops = 2 * rows * width * ffn_local * 2 + 2 * rows * ffn * cols
     return pl.pallas_call(
         functools.partial(expert_kernel, n, tp, across),
@@ -656,7 +778,8 @@
         out_specs=pl.BlockSpec(memory_space=pltpu.VMEM),
         scratch_shapes=[
             pltpu.VMEM((depth, row_count, cols), bf16),
-            pltpu.VMEM((depth, max(1, across - 1), cap, cols), bf16),
+            pltpu.VMEM((depth, row_count, ahead_cols or 128), bf16),
+            pltpu.VMEM((depth, max(1, across - 1), cap, cols + ahead_cols), bf16),
             pltpu.VMEM((n, cap, cols), bf16),
             pltpu.VMEM((row_count, wide * tp), bf16),
             pltpu.VMEM(projection.shape, bf16),
@@ -684,18 +807,20 @@
             dma((n,)),
             dma((n,)),
             dma((n,)),
-            dma((depth + 1, chunks)),
-            dma((depth, chunks)),
-            dma((depth, across)),
-            dma((depth, across)),
-            dma((chips, n)),
-            dma((chips, n)),
-            dma((chips, n)),
-            dma((chips, n)),
-            dma((chips, depth)),
-            dma((chips, depth)),
-            dma((chips, depth)),
-            dma((chips, depth)),
+            dma((2 if ahead_cols else 1,)),
+            dma((1,)),
+            dma((depth + 1, chunks + 1)),
+            dma((depth, chunks + 1)),
+            dma((depth, across, chunks + 1)),
+            dma((depth, across, chunks + 1)),
+            dma((chips, n, chunks + 1)),
+            dma((chips, n, chunks + 1)),
+            dma((chips, n, chunks + 1)),
+            dma((chips, n, chunks + 1)),
+            dma((chips, depth, parts)),
+            dma((chips, depth, parts)),
+            dma((chips, depth, parts)),
+            dma((chips, depth, parts)),
             dma((n,)),
             dma((n,)),
             dma((3,)),

time: 131 us -> 120 us (0.916)
  Pallas kernels: 129 us -> 118 us
    pallas_call x1, Pallas kernels: 129 us -> 118 us  [whole_layer(): pl.pallas_call(functools.partial(expert_kernel, n, tp, across), out_shape...]
where the time goes in v3:
time: 120 us
  Pallas kernels  118 us (98%)
  local copies, waits for them, and re-layouts  1.87 us (2%)
    pallas_call x1, Pallas kernels, whole_layer(): pl.pallas_call(functools.partial(expert_kernel, n, tp, across), out_shape...  118 us

profile of v3, /device:TPU:0, one launch (start us, length us, event | category | flops | bytes accessed | tf_op | source)
XLA Modules:
  0.0 119.7 jit_solution(17712142069281160104)
XLA Ops:
  0.0 117.8 %layer.1 = bf16[256,1024]{1,0:T(8,128)(2,1)} custom-call(bf16[256,512]{1,0:T(8,128)(2,1)} %outer_ref.1, bf16[256,512]{1,0:T(8,128)(2,1)} %inner_ref.1, bf16[256,512]{1,0:T(8,128)(2,1)} %conv_ref.1, bf16[3,512]{1,0:T(4,128)(2,1)} %taps_ref.1, s32[256]{0:T(256)} %docs_ref.1, bf16[256,1024]{1,0:T(8,128)(2,1)} %residual_ref.1, bf16[1024]{0:T(1024)(128)(2,1)} %gain_ref.1, ...), custom_call_target="tpu_custom_call" | custom-call | flops 12884901888 | bytes 12582912 | tf_op jit(solution)/shard_map/layer/pallas_call | solution.py:773
  117.8 1.9 %copy.16 = bf16[256,1024]{1,0:T(8,128)(2,1)} copy(bf16[256,1024]{1,0:T(8,128)(2,1)} %layer.1) | data formatting | bytes 1048576

commit v4 on v3

--- a/solution.py
+++ b/solution.py
@@ -229,7 +229,7 @@
     def send_branch(h):
         region = branch_region(t, h)
         for d in range(1, chips):
-            copy = remote(region, region, by_send.at[d, h], by_recv.at[d, h], (me, chip_at(d)))
+            copy = remote(region, region, by_send.at[d - 1, h], by_recv.at[d - 1, h], (me, chip_at(d)))
             copy.start()
             sends.append(copy)
         copy = remote(region, region, bp_send.at[0, h], bp_recv.at[0, h], (me, partner))
@@ -298,7 +298,7 @@
     for d in range(1, chips):
         source = chip_at(-d)
         for h in (1, 0):
-            branch_arrived(source, by_recv.at[d, h], h).wait_recv()
+            branch_arrived(source, by_recv.at[d - 1, h], h).wait_recv()
             region = branch_region(source, h)
             copy = remote(region, region, bp_send.at[d, h], bp_recv.at[d, h], (me, partner))
             copy.start()
@@ -431,7 +431,7 @@
         region = fan_region(f, home(c), c)
         late = fan_region(f, t, c, True)
         copies = [
-            remote(late, late, y_send.at[e, f, c], y_recv.at[e, f, c], (me, chip_at(e)))
+            remote(late, late, y_send.at[e - 1, f, c], y_recv.at[e - 1, f, c], (me, chip_at(e)))
             for e in range(1, chips if c < chunks else 1)
         ]
         copies.append(
@@ -446,7 +446,6 @@
         ).wait_recv()
         for copy in fan_copies(g, d, c):
             copy.start()
-            sends.append(copy)
 
     def arrive(step, c):
         for g in range(step, min(2 * step, depth - 1) + 1):
@@ -493,19 +492,36 @@
             for copy in fan_copies(g, 0, c):
                 pl.when(is_early(g))(copy.start)
 
-    def relay(g):
+    def relay_pairs(g):
+        pairs = []
         for f in range(g * across, (g + 1) * across):
             for c in range(chunks):
                 for d in range(1, chips):
                     region = fan_region(f, chip_at(-d), c, True)
-                    remote(
-                        region, region, y_send.at[d, f, c], y_recv.at[d, f, c], (me, partner)
-                    ).wait_recv()
-                    copy = remote(
-                        region, region, p_send.at[d, f, c], p_recv.at[d, f, c], (me, partner)
+                    pairs.append(
+                        (
+                            remote(
+                                region,
+                                region,
+                                y_send.at[d - 1, f, c],
+                                y_recv.at[d - 1, f, c],
+                                (me, partner),
+                            ),
+                            remote(
+                                region,
+                                region,
+                                p_send.at[d, f, c],
+                                p_recv.at[d, f, c],
+                                (me, partner),
+                            ),
+                        )
                     )
-                    copy.start()
-                    sends.append(copy)
+        return pairs
+
+    def relay(g):
+        for arrival, copy in relay_pairs(g):
+            arrival.wait_recv()
+            copy.start()
 
     def hid_region(g, index, h):
         return hid.at[
@@ -542,24 +558,27 @@
             if send:
                 send_hidden(g, h)
 
+    def hidden_copies(g, h):
+        region = hid_region(g, t, h)
+        copies = [
+            remote(region, region, hy_send.at[d - 1, g, h], hy_recv.at[d - 1, g, h], (me, chip_at(d)))
+            for d in range(1, chips)
+        ]
+        copies.append(
+            remote(region, region, hp_send.at[0, g, h], hp_recv.at[0, g, h], (me, partner))
+        )
+        return copies
+
     def send_hidden(g, h):
-        region = hid_region(g, t, h)
-        for d in range(1, chips):
-            copy = remote(
-                region, region, hy_send.at[d, g, h], hy_recv.at[d, g, h], (me, chip_at(d))
-            )
+        for copy in hidden_copies(g, h):
             copy.start()
-            sends.append(copy)
-        copy = remote(region, region, hp_send.at[0, g, h], hp_recv.at[0, g, h], (me, partner))
-        copy.start()
-        sends.append(copy)
 
     def relay_hidden(g):
         for h in range(ffn_local // hid_step):
             for d in range(1, chips):
                 region = hid_region(g, chip_at(-d), h)
                 remote(
-                    region, region, hy_send.at[d, g, h], hy_recv.at[d, g, h], (me, partner)
+                    region, region, hy_send.at[d - 1, g, h], hy_recv.at[d - 1, g, h], (me, partner)
                 ).wait_recv()
                 copy = remote(
                     region, region, hp_send.at[d, g, h], hp_recv.at[d, g, h], (me, partner)
@@ -568,6 +587,7 @@
                 sends.append(copy)
 
     down_ready = []
+    returns = []
 
     def down_stage(g):
         for h in range(ffn_local // hid_step):
@@ -604,7 +624,7 @@
                 (group_z(g) * across + lax.rem(x + across - d, across), t),
             )
             copy.start()
-            sends.append(copy)
+            returns.append(copy)
 
     total[...] = jnp.zeros_like(total)
 
@@ -671,6 +691,13 @@
         down_stage(g)
         send_back(g, range(across) if offsets is None else offsets)
 
+    def when_early(g, then, work):
+        if 1 < g:
+            early_here = is_early(g)
+            pl.when(early_here if then else jnp.logical_not(early_here))(work)
+        elif not then:
+            work()
+
     for s in range(1, depth):
         arrive(s, 0)
         if s == 1:
@@ -693,6 +720,8 @@
             release(s + 1)
         else:
             down_part(s - 2, [0])
+            for c in range(pieces):
+                when_early(s, True, functools.partial(fan_across, s, c))
             for c in range(1, chunks):
                 arrive(s, c)
             up_part(s - 1)
@@ -701,20 +730,36 @@
             send_back(s - 2, range(1, across))
             select_early(s + 1)
             for c in range(pieces):
-                fan_across(s, c)
+                when_early(s, False, functools.partial(fan_across, s, c))
             release(s + 1)
+    when_early(last, True, functools.partial(up_part, last, last > 0))
     if last > 1:
         down_part(last - 1)
-    up_part(last, last > 0)
+    when_early(last, False, functools.partial(up_part, last, last > 0))
     for h in range(ffn_local // hid_step):
         send_hidden(0, h)
     if last > 0:
         down_part(last)
     down_part(0)
 
+    for copy in sends:
+        copy.wait_send()
+    for started, copy in guarded:
+        pl.when(started)(copy.wait_send)
+    for g in range(depth):
+        for _, copy in relay_pairs(g):
+            copy.wait_send()
+        for h in range(ffn_local // hid_step):
+            for copy in hidden_copies(g, h):
+                copy.wait_send()
+        for d in range(1, across):
+            for c in range(pieces):
+                for copy in fan_copies(g, d, c):
+                    copy.wait_send()
+
     lanes = lax.broadcasted_iota(jnp.int32, (row_count, 128), 1)
     slot_lanes = lax.broadcasted_iota(jnp.int32, (row_count, cap), 1).astype(jnp.float32)
-    turns = [*range(1, last), 0, last] if last > 0 else [0]
+    turns = [*range(1, last - 1), last, last - 1, 0] if last > 1 else [*range(last, -1, -1)]
     for turn, g in enumerate(turns):
         chosen = []
         for d in range(across):
@@ -746,10 +791,8 @@
             return carry
 
         lax.fori_loop(0, cols // step, combine, 0)
-    for copy in sends:
+    for copy in returns:
         copy.wait_send()
-    for started, copy in guarded:
-        pl.when(started)(copy.wait_send)
 
 
 def whole_layer(blocks, weights):
@@ -811,22 +854,22 @@
             dma((1,)),
             dma((depth + 1, chunks + 1)),
             dma((depth, chunks + 1)),
-            dma((depth, across, chunks + 1)),
-            dma((depth, across, chunks + 1)),
+            dma((depth, max(1, across - 1), chunks + 1)),
+            dma((depth, max(1, across - 1), chunks + 1)),
+            dma((max(1, chips - 1), n, chunks)),
+            dma((max(1, chips - 1), n, chunks)),
             dma((chips, n, chunks + 1)),
             dma((chips, n, chunks + 1)),
-            dma((chips, n, chunks + 1)),
-            dma((chips, n, chunks + 1)),
-            dma((chips, depth, parts)),
-            dma((chips, depth, parts)),
+            dma((max(1, chips - 1), depth, parts)),
+            dma((max(1, chips - 1), depth, parts)),
             dma((chips, depth, parts)),
             dma((chips, depth, parts)),
             dma((n,)),
             dma((n,)),
             dma((3,)),
             dma((3,)),
-            dma((chips, 2)),
-            dma((chips, 2)),
+            dma((max(1, chips - 1), 2)),
+            dma((max(1, chips - 1), 2)),
             dma((chips, 2)),
             dma((chips, 2)),
             dma((tp,)),

time: 120 us -> 118 us (0.983)
  Pallas kernels: 118 us -> 116 us
    pallas_call x1, Pallas kernels: 118 us -> 116 us  [whole_layer(): pl.pallas_call(functools.partial(expert_kernel, n, tp, across), out_shape...]
where the time goes in v4:
time: 118 us
  Pallas kernels  116 us (98%)
  local copies, waits for them, and re-layouts  1.87 us (2%)
    pallas_call x1, Pallas kernels, whole_layer(): pl.pallas_call(functools.partial(expert_kernel, n, tp, across), out_shape...  116 us

profile of v4, /device:TPU:0, one launch (start us, length us, event | category | flops | bytes accessed | tf_op | source)
XLA Modules:
  0.0 118.0 jit_solution(6433459254472572251)
XLA Ops:
  0.0 116.1 %layer.1 = bf16[256,1024]{1,0:T(8,128)(2,1)} custom-call(bf16[256,512]{1,0:T(8,128)(2,1)} %outer_ref.1, bf16[256,512]{1,0:T(8,128)(2,1)} %inner_ref.1, bf16[256,512]{1,0:T(8,128)(2,1)} %conv_ref.1, bf16[3,512]{1,0:T(4,128)(2,1)} %taps_ref.1, s32[256]{0:T(256)} %docs_ref.1, bf16[256,1024]{1,0:T(8,128)(2,1)} %residual_ref.1, bf16[1024]{0:T(1024)(128)(2,1)} %gain_ref.1, ...), custom_call_target="tpu_custom_call" | custom-call | flops 12884901888 | bytes 12582912 | tf_op jit(solution)/shard_map/layer/pallas_call | solution.py:816
  116.1 1.9 %copy.16 = bf16[256,1024]{1,0:T(8,128)(2,1)} copy(bf16[256,1024]{1,0:T(8,128)(2,1)} %layer.1) | data formatting | bytes 1048576

commit v5 on v4

--- a/solution.py
+++ b/solution.py
@@ -612,7 +612,7 @@
         lax.fori_loop(0, cols // step, tile, 0)
 
     def send_back(g, offsets):
-        for d in offsets:
+        for d in reversed(offsets):
             if g == 0 and d == 0:
                 continue
             k = g * across + d

time: 118 us -> 117 us (level)
    pallas_call x1, Pallas kernels: 116 us -> 115 us  [whole_layer(): pl.pallas_call(functools.partial(expert_kernel, n, tp, across), out_shape...]
where the time goes in v5:
time: 117 us; the launch traced here: 116 us
  Pallas kernels  115 us (98%)
  local copies, waits for them, and re-layouts  1.87 us (2%)
    pallas_call x1, Pallas kernels, whole_layer(): pl.pallas_call(functools.partial(expert_kernel, n, tp, across), out_shape...  115 us

profile of v5, /device:TPU:0, one launch (start us, length us, event | category | flops | bytes accessed | tf_op | source)
XLA Modules:
  0.0 116.5 jit_solution(4903416513359129840)
XLA Ops:
  0.0 114.6 %layer.1 = bf16[256,1024]{1,0:T(8,128)(2,1)} custom-call(bf16[256,512]{1,0:T(8,128)(2,1)} %outer_ref.1, bf16[256,512]{1,0:T(8,128)(2,1)} %inner_ref.1, bf16[256,512]{1,0:T(8,128)(2,1)} %conv_ref.1, bf16[3,512]{1,0:T(4,128)(2,1)} %taps_ref.1, s32[256]{0:T(256)} %docs_ref.1, bf16[256,1024]{1,0:T(8,128)(2,1)} %residual_ref.1, bf16[1024]{0:T(1024)(128)(2,1)} %gain_ref.1, ...), custom_call_target="tpu_custom_call" | custom-call | flops 12884901888 | bytes 12582912 | tf_op jit(solution)/shard_map/layer/pallas_call | solution.py:816
  114.6 1.9 %copy.16 = bf16[256,1024]{1,0:T(8,128)(2,1)} copy(bf16[256,1024]{1,0:T(8,128)(2,1)} %layer.1) | data formatting | bytes 1048576
